TPU v7x, 32 devices: a whole 2x2x4 slice. The times are simulated.
32 devices in a mesh: sp: 8 (over z, x), tp: 4 (over y, core).
Axes of the slice: x: 2, y: 2, z: 4, core: 2. Of those that a mesh axis runs over, the one named last changes fastest.
Arguments:
- residual: bfloat16 [4096, 2048], P('sp'), may hold values from -80 to 80
- queries: bfloat16 [4096, 1024], P('sp', 'tp'), may hold values from -260 to 260
- keys: bfloat16 [4096, 512], P('sp', 'tp'), may hold values from -7 to 7
- values: bfloat16 [4096, 512], P('sp', 'tp'), may hold values from -12 to 12
- documents: int32 [4096], P('sp'), may hold values from 0 to 3, never falling along the last dimension, each value on 1 to 3072 neighbouring positions
- sinks: float32 [16], P('tp'), may hold values from 1 to 6
- out_weight: bfloat16 [1024, 2048], P('tp'), may hold values from -0.5 to 0.5
- norm_gain: float32 [2048], replicated, may hold values from 0.1 to 1.9
- gate_weight: bfloat16 [2048, 5632], P('sp', 'tp'), may hold values from -0.125 to 0.125
- up_weight: bfloat16 [2048, 5632], P('sp', 'tp'), may hold values from -0.125 to 0.125
- down_weight: bfloat16 [2048, 5632], P('sp', 'tp'), may hold values from -0.078125 to 0.078125
Outputs:
- mixed: bfloat16 [4096, 2048], P('sp', 'tp')
Inputs may be any that keep to these rules, and one draw needn't show every extreme that they name: `documents`: document numbers never fall along the positions; a document holds at most 3072 positions.
All inputs are finite; a program needn't handle non-finite values.
Results may differ from a plain program's by a relative error of at most 0.01.
Values may be sent and summed in bfloat16 or wider, within the bound.
A program may use at most 64 MiB of HBM per device.

v0:
```python
import functools

import jax
import jax.numpy as jnp
from jax import lax
from jax.experimental import pallas as pl
from jax.experimental.pallas import tpu as pltpu
from jax.sharding import PartitionSpec as P

HEAD_DIM = 64
WINDOW = 128
GROUP = 2


neg_big = -1e30
norm_eps = 1e-05


def from_behind(shard, axis, by):
    length = lax.axis_size(axis)
    pairs = [(i, i + by) for i in range(length) if 0 <= i + by < length]
    return lax.ppermute(shard, axis, pairs)


def attend(queries, keys, values, documents, sinks, tail_keys, tail_values, tail_docs, offset):
    rows_here = queries.shape[0]
    block_count = rows_here // WINDOW
    kv_here = keys.shape[1] // HEAD_DIM
    q_blocks = queries.reshape(block_count, WINDOW, kv_here, GROUP, HEAD_DIM)
    k_blocks = keys.reshape(block_count, WINDOW, kv_here, HEAD_DIM)
    v_blocks = values.reshape(block_count, WINDOW, kv_here, HEAD_DIM)
    k_prev = jnp.concatenate(
        [tail_keys.reshape(1, WINDOW, kv_here, HEAD_DIM), k_blocks[:-1]], axis=0
    )
    v_prev = jnp.concatenate(
        [tail_values.reshape(1, WINDOW, kv_here, HEAD_DIM), v_blocks[:-1]], axis=0
    )
    k_band = jnp.concatenate([k_prev, k_blocks], axis=1)
    v_band = jnp.concatenate([v_prev, v_blocks], axis=1)
    doc_own = documents.astype(jnp.float32).reshape(block_count, WINDOW)
    doc_prev = jnp.concatenate(
        [tail_docs.astype(jnp.float32).reshape(1, WINDOW), doc_own[:-1]], axis=0
    )
    doc_band = jnp.concatenate([doc_prev, doc_own], axis=1)
    row_idx = jnp.arange(WINDOW, dtype=jnp.int32)
    col_idx = jnp.arange(2 * WINDOW, dtype=jnp.int32)
    first = offset + jnp.arange(block_count, dtype=jnp.int32) * WINDOW
    q_pos = first[:, None] + row_idx[None, :]
    k_pos = first[:, None] - WINDOW + col_idx[None, :]
    distance = q_pos[:, :, None] - k_pos[:, None, :]
    visible = (
        (distance >= 0)
        & (distance < WINDOW)
        & (k_pos[:, None, :] >= 0)
        & (doc_own[:, :, None] == doc_band[:, None, :])
    )
    scores = jnp.einsum(
        "nikgd,njkd->nkgij", q_blocks, k_band, preferred_element_type=jnp.float32
    ) * HEAD_DIM ** (-0.5)
    scores = jnp.where(visible[:, None, None], scores, neg_big)
    sink_logit = sinks.reshape(1, kv_here, GROUP, 1, 1)
    row_max = jnp.maximum(scores.max(-1, keepdims=True), sink_logit)
    expo = jnp.where(visible[:, None, None], jnp.exp(scores - row_max), 0.0)
    denom_sum = expo.sum(-1, keepdims=True) + jnp.exp(sink_logit - row_max)
    weights = (expo / denom_sum).astype(jnp.bfloat16)
    mixed = jnp.einsum("nkgij,njkd->nikgd", weights, v_band, preferred_element_type=jnp.float32)
    return mixed.reshape(rows_here, kv_here * GROUP * HEAD_DIM).astype(jnp.bfloat16)


def on_device(
    residual,
    queries,
    keys,
    values,
    documents,
    sinks,
    out_weight,
    norm_gain,
    gate_weight,
    up_weight,
    down_weight,
):
    rows_here = queries.shape[0]
    offset = lax.axis_index("sp") * rows_here
    doc_tail = documents[rows_here - WINDOW :].astype(jnp.bfloat16)
    tail_keys, tail_values, tail_docs = from_behind(
        (keys[rows_here - WINDOW :], values[rows_here - WINDOW :], doc_tail), "sp", 1
    )
    attended = attend(
        queries, keys, values, documents, sinks, tail_keys, tail_values, tail_docs, offset
    )
    model_width = residual.shape[1]
    col_count = model_width // lax.axis_size("tp")
    col_first = lax.axis_index("tp") * col_count
    full_term = jnp.dot(attended, out_weight, preferred_element_type=jnp.float32)
    projected = lax.psum(full_term.astype(jnp.bfloat16), "tp").astype(jnp.float32)
    after_full = (residual.astype(jnp.float32) + projected).astype(jnp.bfloat16)
    after_f = after_full.astype(jnp.float32)
    inv_rms = lax.rsqrt(jnp.mean(after_f * after_f, axis=1, keepdims=True) + norm_eps)
    normed = (after_f * inv_rms * norm_gain[None, :]).astype(jnp.bfloat16)
    after = lax.dynamic_slice_in_dim(after_full, col_first, col_count, 1)
    gate_act = jnp.dot(
        normed,
        lax.all_gather(gate_weight, "sp", axis=0, tiled=True),
        preferred_element_type=jnp.float32,
    )
    up_act = jnp.dot(
        normed,
        lax.all_gather(up_weight, "sp", axis=0, tiled=True),
        preferred_element_type=jnp.float32,
    )
    down_full = lax.all_gather(down_weight, "sp", axis=0, tiled=True)
    hidden = (jax.nn.silu(gate_act) * up_act).astype(jnp.bfloat16)
    summed = lax.psum_scatter(
        lax.dot_general(
            down_full, hidden, (((1,), (1,)), ((), ())), preferred_element_type=jnp.float32
        ).astype(jnp.bfloat16),
        "tp",
        scatter_dimension=0,
        tiled=True,
    ).astype(jnp.float32)
    return (after.astype(jnp.float32) + summed.T).astype(jnp.bfloat16)


MESH = pl.DeviceIdType.MESH
NT = (((1,), (1,)), ((), ()))


def dot(a, b, dims=(((1,), (0,)), ((), ()))):
    return lax.dot_general(a, b, dims, preferred_element_type=jnp.float32)


def kernel(
    S, T,
    res_hbm, q_ref, k_ref, v_ref, doc_ref, sink_ref, ow_hbm, gain_ref, g_hbm, u_hbm, d_hbm,
    out_ref,
    G, kx, vx, dx, att, res_v, ow_v, psend, precv, after, normed, ga, ua, hidden, dsend, drecv,
    w_send, w_recv, tail_send, tail_recv, loc, p_send, p_recv, a_send, a_recv, d_send, d_recv,
):
    s = lax.axis_index("sp")
    t = lax.axis_index("tp")
    R = q_ref.shape[0]
    D = gain_ref.shape[1]
    C = D // T
    K = D // S
    F = g_hbm.shape[1]
    HK = K // 2
    PER = C // K
    z, x = s // 2, s % 2
    up, down_z = (z + 1) % 4, (z + 3) % 4
    nb_z = z + 1 - 2 * (z % 2)
    f1_z = 2 - z // 2
    f2_z = 3 - 3 * (z // 2)
    zp, zm, xp = up * 2 + x, down_z * 2 + x, z * 2 + 1 - x
    nb, f1, f2 = nb_z * 2 + x, f1_z * 2 + x, f2_z * 2 + x
    nb_x, f1_x, f2_x = nb_z * 2 + 1 - x, f1_z * 2 + 1 - x, f2_z * 2 + 1 - x
    far = ((z + 2) % 4) * 2 + x
    end = (3 - z) * 2 + x
    has_up, has_down = z < 3, z > 0
    after_s = (s + 1) % S
    before_s = (s + S - 1) % S

    weights = (g_hbm, u_hbm, d_hbm)
    local = [
        pltpu.make_async_copy(weights[m], G.at[m, s], loc.at[m]) for m in range(3)
    ]
    local.append(pltpu.make_async_copy(ow_hbm, ow_v, loc.at[3]))
    local.append(pltpu.make_async_copy(
        res_hbm.at[:, pl.ds(pl.multiple_of(t * C, C), C)], res_v, loc.at[4]))
    for c in (local[3], local[4], local[0], local[1], local[2]):
        c.start()

    barrier = pltpu.get_barrier_semaphore()
    peers = [(zp, t), (zm, t), (xp, t), (after_s, t), (before_s, t)]
    peers += [(s, (t + d) % T) for d in range(1, T)]
    for p in peers:
        pl.semaphore_signal(barrier, inc=1, device_id=p, device_id_type=MESH)
    pl.semaphore_wait(barrier, len(peers))

    started = []

    tails = []
    for i, (a, b) in enumerate((
        (k_ref.at[pl.ds(R - WINDOW, WINDOW)], kx.at[pl.ds(0, WINDOW)]),
        (v_ref.at[pl.ds(R - WINDOW, WINDOW)], vx.at[pl.ds(0, WINDOW)]),
        (doc_ref.at[pl.ds(doc_ref.shape[0] - 8, 8)], dx.at[pl.ds(0, 8)]),
    )):
        c = pltpu.make_async_remote_copy(
            src_ref=a, dst_ref=b, send_sem=tail_send.at[i], recv_sem=tail_recv.at[i],
            device_id=(after_s, t), device_id_type=MESH)
        c.start()
        tails.append(c)

    target = (zp, zm, xp, nb)
    count = [0, 0, 0, 0]

    def when(cond, f):
        if cond is None:
            f()
        else:
            pl.when(cond)(f)

    def send(link, m, src, h, own=False, cond=None):
        part = pl.ds(h * HK, HK)
        place = G.at[m, src, part]
        c = pltpu.make_async_remote_copy(
            src_ref=weights[m].at[part] if own else place, dst_ref=place,
            send_sem=w_send.at[link, count[link]], recv_sem=w_recv.at[m, src, h],
            device_id=(target[link], t), device_id_type=MESH)
        count[link] += 1
        when(cond, c.start)
        started.append((cond, c))

    def recv(m, src, h, cond=None):
        place = G.at[m, src, pl.ds(h * HK, HK)]
        c = pltpu.make_async_remote_copy(
            src_ref=place, dst_ref=place, send_sem=w_send.at[0, 0],
            recv_sem=w_recv.at[m, src, h], device_id=(xp, t), device_id_type=MESH)
        when(cond, c.wait_recv)

    GU = ((0, 0), (0, 1), (1, 0), (1, 1))
    DN = ((2, 0), (2, 1))

    def own_z(units):
        for m, h in units:
            send(0, m, s, h, own=True, cond=has_up)
            send(1, m, s, h, own=True, cond=has_down)

    def own_x(units):
        for m, h in units:
            send(2, m, s, h, own=True)

    def near(units):
        for m, h in units:
            recv(m, zp, h, has_up)
            send(1, m, zp, h, cond=has_up & has_down)
            recv(m, zm, h, has_down)
            send(0, m, zm, h, cond=has_up & has_down)
            if h == 1:
                send(2, m, nb, h)

    def middle(units):
        for m, h in units:
            recv(m, far, h)
            send(1, m, far, h, cond=z == 1)
            send(0, m, far, h, cond=z == 2)
            send(2, m, f1, h)

    def farthest(units):
        for m, h in units:
            recv(m, end, h, (z == 0) | (z == 3))
            send(2, m, f2, h)

    def extra(units):
        for m, h in units:
            recv(m, xp, h)
            if h == 0:
                send(3, m, xp, h)

    for m, h in GU:
        send(0, m, s, h, own=True, cond=has_up)
        send(1, m, s, h, own=True, cond=has_down)
        send(2, m, s, h, own=True)

    kx[pl.ds(WINDOW, R), :] = k_ref[...]
    vx[pl.ds(WINDOW, R), :] = v_ref[...]
    dx[pl.ds(8, doc_ref.shape[0]), :] = doc_ref[...]
    for c in tails:
        c.wait_recv()
    heads = q_ref.shape[1] // HEAD_DIM

    def block(b, carry):
        rows = pl.ds(pl.multiple_of(b * WINDOW, WINDOW), WINDOW)
        band = pl.ds(pl.multiple_of(b * WINDOW, WINDOW), 2 * WINDOW)
        prev = dx[pl.ds(pl.multiple_of(b * 8, 8), 8), :][0:1].astype(jnp.float32)
        own = dx[pl.ds(pl.multiple_of(b * 8 + 8, 8), 8), :][0:1].astype(jnp.float32)
        doc_q = jnp.broadcast_to(own, (WINDOW, WINDOW)).T
        i = lax.broadcasted_iota(jnp.int32, (WINDOW, WINDOW), 0)
        j = lax.broadcasted_iota(jnp.int32, (WINDOW, WINDOW), 1)
        first = s * R + b * WINDOW - WINDOW
        see_prev = (j > i) & (doc_q == prev) & (first + j >= 0)
        see_own = (j <= i) & (doc_q == own)
        visible = jnp.concatenate(
            [see_prev.astype(jnp.float32), see_own.astype(jnp.float32)], axis=1) > 0.5
        for h in range(heads):
            kv = h // GROUP
            cols = slice(kv * HEAD_DIM, (kv + 1) * HEAD_DIM)
            q = q_ref[rows, h * HEAD_DIM:(h + 1) * HEAD_DIM]
            scores = dot(q, kx[band, cols], NT) * HEAD_DIM ** (-0.5)
            scores = jnp.where(visible, scores, neg_big)
            sink = sink_ref[h]
            row_max = jnp.maximum(scores.max(-1, keepdims=True), sink)
            expo = jnp.where(visible, jnp.exp(scores - row_max), 0.0)
            total = expo.sum(-1, keepdims=True) + jnp.exp(sink - row_max)
            w = (expo / total).astype(jnp.bfloat16)
            att[rows, h * HEAD_DIM:(h + 1) * HEAD_DIM] = dot(w, vx[band, cols]).astype(jnp.bfloat16)
        return carry

    lax.fori_loop(0, R // WINDOW, block, 0)

    local[3].wait()
    reach = [(t + d) % T for d in (2, 1, 3)]
    psent = []
    for n, owner in enumerate(reach + [t]):
        cols = pl.ds(pl.multiple_of(owner * C, C), C)
        value = dot(att[...], ow_v[:, cols]).astype(jnp.bfloat16)
        if n == T - 1:
            precv[t] = value
        else:
            psend[owner] = value
            c = pltpu.make_async_remote_copy(
                src_ref=psend.at[owner], dst_ref=precv.at[t], send_sem=p_send.at[n],
                recv_sem=p_recv.at[t], device_id=(s, owner), device_id_type=MESH)
            c.start()
            psent.append(c)

    def recv_block(buf, sems, source):
        pltpu.make_async_remote_copy(
            src_ref=buf.at[source], dst_ref=buf.at[source], send_sem=p_send.at[0],
            recv_sem=sems.at[source], device_id=(s, (t + 1) % T), device_id_type=MESH).wait_recv()

    near(GU)

    local[4].wait()
    for owner in reach:
        recv_block(precv, p_recv, owner)
    total = precv[0].astype(jnp.float32)
    for i in range(1, T):
        total += precv[i].astype(jnp.float32)
    after[t] = (res_v[...].astype(jnp.float32) + total).astype(jnp.bfloat16)
    asent = []
    for n, peer in enumerate(reach):
        c = pltpu.make_async_remote_copy(
            src_ref=after.at[t], dst_ref=after.at[t], send_sem=a_send.at[n],
            recv_sem=a_recv.at[t], device_id=(s, peer), device_id_type=MESH)
        c.start()
        asent.append(c)

    middle(GU)
    extra(GU)
    own_z(DN)
    farthest(GU[:2])

    for peer in reach:
        recv_block(after, a_recv, peer)

    def norm(r, carry):
        rows = pl.ds(pl.multiple_of(r * 64, 64), 64)
        parts = [after[i, rows, :].astype(jnp.float32) for i in range(T)]
        square = (parts[0] * parts[0]).sum(-1, keepdims=True)
        for p in parts[1:]:
            square += (p * p).sum(-1, keepdims=True)
        inv = lax.rsqrt(square / D + norm_eps)
        for i in range(T):
            n = (parts[i] * inv * gain_ref[:, i * C:(i + 1) * C]).astype(jnp.bfloat16)
            for j in range(PER):
                normed[i * PER + j, rows, :] = n[:, j * K:(j + 1) * K]
        return carry

    lax.fori_loop(0, R // 64, norm, 0)

    TM = 128

    def gate_up(src, begin=False):
        def tile(r, carry):
            rows = pl.ds(pl.multiple_of(r * TM, TM), TM)
            a = normed[src, rows, :]
            for m, acc in ((0, ga), (1, ua)):
                value = dot(a, G[m, src])
                if begin:
                    acc[rows, :] = value
                else:
                    acc[rows, :] += value
            return carry
        lax.fori_loop(0, R // TM, tile, 0)

    local[0].wait()
    local[1].wait()
    gate_up(s, True)
    gate_up(nb)
    farthest(GU[2:])
    own_x(DN)
    gate_up(xp)
    gate_up(f1)
    gate_up(f2)
    for src in (nb_x, f1_x, f2_x):
        for m, h in GU:
            recv(m, src, h)
        gate_up(src)

    def act(r, carry):
        rows = pl.ds(pl.multiple_of(r * 32, 32), 32)
        g = ga[rows, :]
        hidden[rows, :] = (g / (1.0 + jnp.exp(-g)) * ua[rows, :]).astype(jnp.bfloat16)
        return carry

    lax.fori_loop(0, R // 32, act, 0)

    def down_copy(src, h):
        owner = src // PER
        return owner, pltpu.make_async_remote_copy(
            src_ref=dsend.at[src, h], dst_ref=drecv.at[t, src % PER, h],
            send_sem=d_send.at[src, h], recv_sem=d_recv.at[t, src % PER, h],
            device_id=(s, owner), device_id_type=MESH)

    def down(src, h):
        value = dot(hidden[...], G[2, src, h * HK:(h + 1) * HK, :], NT).astype(jnp.bfloat16)
        owner, c = down_copy(src, h)

        @pl.when(owner != t)
        def _():
            dsend[src, h] = value
            c.start()

        @pl.when(owner == t)
        def _():
            drecv[t, src % PER, h] = value

    local[2].wait()
    near(DN)
    down(s, 0)
    down(s, 1)
    down(nb, 0)
    down(nb, 1)
    middle(DN)
    extra(DN)
    for src in (xp, f1):
        for h in (0, 1):
            down(src, h)
    for h in (1, 0):
        if h == 0:
            farthest(DN)
        recv(2, nb_x, h)
        down(nb_x, h)
    for src in (f2, f1_x, f2_x):
        for h in (0, 1):
            if src is not f2:
                recv(2, src, h)
            down(src, h)

    for i in range(PER):
        for h in (0, 1):
            for peer in reach:
                pltpu.make_async_remote_copy(
                    src_ref=drecv.at[peer, i, h], dst_ref=drecv.at[peer, i, h],
                    send_sem=d_send.at[0, 0], recv_sem=d_recv.at[peer, i, h],
                    device_id=(s, (t + 1) % T), device_id_type=MESH).wait_recv()
            total = drecv[0, i, h].astype(jnp.float32)
            for n in range(1, T):
                total += drecv[n, i, h].astype(jnp.float32)
            cols = slice((i * 2 + h) * HK, (i * 2 + h + 1) * HK)
            out_ref[:, cols] = (after[t, :, cols].astype(jnp.float32) + total).astype(jnp.bfloat16)

    for cond, c in started:
        when(cond, c.wait_send)
    for c in tails + psent + asent:
        c.wait_send()
    for src in range(S):
        for h in (0, 1):
            owner, c = down_copy(src, h)

            @pl.when(owner != t)
            def _():
                c.wait_send()


def fused(residual, queries, keys, values, documents, sinks, out_weight, norm_gain, gate_weight, up_weight, down_weight):
    S, T = lax.axis_size("sp"), lax.axis_size("tp")
    R, D = residual.shape
    F = gate_weight.shape[1]
    C, K = D // T, D // S
    blocks = R // WINDOW
    docs = jnp.broadcast_to(documents.reshape(blocks, 1, WINDOW), (blocks, 8, WINDOW)).reshape(blocks * 8, WINDOW)
    bf, f32 = jnp.bfloat16, jnp.float32
    vm, hbm = pl.BlockSpec(memory_space=pltpu.VMEM), pl.BlockSpec(memory_space=pl.ANY)
    dma = pltpu.SemaphoreType.DMA
    scratch = [
        pltpu.VMEM((3, S, K, F), bf),
        pltpu.VMEM((R + WINDOW, keys.shape[1]), bf),
        pltpu.VMEM((R + WINDOW, keys.shape[1]), bf),
        pltpu.VMEM((blocks * 8 + 8, WINDOW), jnp.int32),
        pltpu.VMEM((R, queries.shape[1]), bf),
        pltpu.VMEM((R, C), bf),
        pltpu.VMEM(out_weight.shape, bf),
        pltpu.VMEM((T, R, C), bf),
        pltpu.VMEM((T, R, C), bf),
        pltpu.VMEM((T, R, C), bf),
        pltpu.VMEM((S, R, K), bf),
        pltpu.VMEM((R, F), f32),
        pltpu.VMEM((R, F), f32),
        pltpu.VMEM((R, F), bf),
        pltpu.VMEM((S, 2, R, K // 2), bf),
        pltpu.VMEM((T, C // K, 2, R, K // 2), bf),
        dma((4, 21)), dma((3, S, 2)), dma((3,)), dma((3,)), dma((5,)),
        dma((T,)), dma((T,)), dma((T,)), dma((T,)), dma((S, 2)), dma((T, C // K, 2)),
    ]
    return pl.pallas_call(
        functools.partial(kernel, S, T),
        out_shape=jax.ShapeDtypeStruct((R, C), bf),
        in_specs=[hbm, vm, vm, vm, vm, pl.BlockSpec(memory_space=pltpu.SMEM), hbm, vm, hbm, hbm, hbm],
        out_specs=vm,
        scratch_shapes=scratch,
        compiler_params=pltpu.CompilerParams(
            collective_id=0, has_side_effects=True, vmem_limit_bytes=60 * 2**20),
    )(residual, queries, keys, values, docs, sinks, out_weight, norm_gain.reshape(1, D),
      gate_weight, up_weight, down_weight)


def line_of_four_pairs(mesh):
    return mesh.shape["sp"] == 8 and mesh.shape["tp"] == 4


def solution(mesh):
    return jax.shard_map(
        fused if line_of_four_pairs(mesh) else on_device,
        mesh=mesh,
        in_specs=(
            P("sp", None),
            P("sp", "tp"),
            P("sp", "tp"),
            P("sp", "tp"),
            P("sp"),
            P("tp"),
            P("tp", None),
            P(),
            P("sp", "tp"),
            P("sp", "tp"),
            P("sp", "tp"),
        ),
        out_specs=P("sp", "tp"),
        check_vma=False,
    )
```

profile of v0, /device:TPU:0, one launch (start us, length us, event | category | flops | bytes accessed | tf_op | source)
XLA Modules:
  0.0 193.3 jit_solution(16332426959118643296)
XLA Ops:
  0.0 0.0 copy-start
  0.0 0.7 copy-done
  0.7 0.6 broadcast_bitcast_fusion.doc_ref
  1.3 190.1 %shard_map.109 = bf16[512,512]{1,0:T(8,128)(2,1)} custom-call(bf16[512,2048]{1,0:T(8,128)(2,1)} %res_hbm.1, bf16[512,256]{1,0:T(8,128)(2,1)} %q_ref.1, bf16[512,128]{1,0:T(8,128)(2,1)} %k_ref.1, bf16[512,128]{1,0:T(8,128)(2,1)} %v_ref.1, s32[32,128]{1,0:T(8,128)} %broadcast_bitcast_fusion.doc_ref, f32[4]{0:T(128)} %sink_ref.1, bf16[256,2048]{1,0:T(8,128)(2,1)} %ow_hbm.1, ...), custom_call_target="tpu_custom_call" | custom-call | tf_op jit(solution)/shard_map/pallas_call | solution.py:497
  191.4 1.9 copy.13
Async XLA Ops:
  0.0 0.7 copy-start
where the time goes:
time: 195 us; the launch traced here: 193 us
  Pallas kernels  190 us (97%)
  local copies, waits for them, and re-layouts  3.16 us (2%)
    pallas_call x1, Pallas kernels, fused(): pl.pallas_call(functools.partial(kernel, S, T), out_shape=jax.ShapeDtypeS...  190 us

commit v1 on v0

v1 whole, which is shorter than its diff:
```python
import functools

import jax
import jax.numpy as jnp
from jax import lax
from jax.experimental import pallas as pl
from jax.experimental.pallas import tpu as pltpu
from jax.sharding import PartitionSpec as P

HEAD_DIM = 64
WINDOW = 128
GROUP = 2


neg_big = -1e30
norm_eps = 1e-05


def from_behind(shard, axis, by):
    length = lax.axis_size(axis)
    pairs = [(i, i + by) for i in range(length) if 0 <= i + by < length]
    return lax.ppermute(shard, axis, pairs)


def attend(queries, keys, values, documents, sinks, tail_keys, tail_values, tail_docs, offset):
    rows_here = queries.shape[0]
    block_count = rows_here // WINDOW
    kv_here = keys.shape[1] // HEAD_DIM
    q_blocks = queries.reshape(block_count, WINDOW, kv_here, GROUP, HEAD_DIM)
    k_blocks = keys.reshape(block_count, WINDOW, kv_here, HEAD_DIM)
    v_blocks = values.reshape(block_count, WINDOW, kv_here, HEAD_DIM)
    k_prev = jnp.concatenate(
        [tail_keys.reshape(1, WINDOW, kv_here, HEAD_DIM), k_blocks[:-1]], axis=0
    )
    v_prev = jnp.concatenate(
        [tail_values.reshape(1, WINDOW, kv_here, HEAD_DIM), v_blocks[:-1]], axis=0
    )
    k_band = jnp.concatenate([k_prev, k_blocks], axis=1)
    v_band = jnp.concatenate([v_prev, v_blocks], axis=1)
    doc_own = documents.astype(jnp.float32).reshape(block_count, WINDOW)
    doc_prev = jnp.concatenate(
        [tail_docs.astype(jnp.float32).reshape(1, WINDOW), doc_own[:-1]], axis=0
    )
    doc_band = jnp.concatenate([doc_prev, doc_own], axis=1)
    row_idx = jnp.arange(WINDOW, dtype=jnp.int32)
    col_idx = jnp.arange(2 * WINDOW, dtype=jnp.int32)
    first = offset + jnp.arange(block_count, dtype=jnp.int32) * WINDOW
    q_pos = first[:, None] + row_idx[None, :]
    k_pos = first[:, None] - WINDOW + col_idx[None, :]
    distance = q_pos[:, :, None] - k_pos[:, None, :]
    visible = (
        (distance >= 0)
        & (distance < WINDOW)
        & (k_pos[:, None, :] >= 0)
        & (doc_own[:, :, None] == doc_band[:, None, :])
    )
    scores = jnp.einsum(
        "nikgd,njkd->nkgij", q_blocks, k_band, preferred_element_type=jnp.float32
    ) * HEAD_DIM ** (-0.5)
    scores = jnp.where(visible[:, None, None], scores, neg_big)
    sink_logit = sinks.reshape(1, kv_here, GROUP, 1, 1)
    row_max = jnp.maximum(scores.max(-1, keepdims=True), sink_logit)
    expo = jnp.where(visible[:, None, None], jnp.exp(scores - row_max), 0.0)
    denom_sum = expo.sum(-1, keepdims=True) + jnp.exp(sink_logit - row_max)
    weights = (expo / denom_sum).astype(jnp.bfloat16)
    mixed = jnp.einsum("nkgij,njkd->nikgd", weights, v_band, preferred_element_type=jnp.float32)
    return mixed.reshape(rows_here, kv_here * GROUP * HEAD_DIM).astype(jnp.bfloat16)


def on_device(
    residual,
    queries,
    keys,
    values,
    documents,
    sinks,
    out_weight,
    norm_gain,
    gate_weight,
    up_weight,
    down_weight,
):
    rows_here = queries.shape[0]
    offset = lax.axis_index("sp") * rows_here
    doc_tail = documents[rows_here - WINDOW :].astype(jnp.bfloat16)
    tail_keys, tail_values, tail_docs = from_behind(
        (keys[rows_here - WINDOW :], values[rows_here - WINDOW :], doc_tail), "sp", 1
    )
    attended = attend(
        queries, keys, values, documents, sinks, tail_keys, tail_values, tail_docs, offset
    )
    model_width = residual.shape[1]
    col_count = model_width // lax.axis_size("tp")
    col_first = lax.axis_index("tp") * col_count
    full_term = jnp.dot(attended, out_weight, preferred_element_type=jnp.float32)
    projected = lax.psum(full_term.astype(jnp.bfloat16), "tp").astype(jnp.float32)
    after_full = (residual.astype(jnp.float32) + projected).astype(jnp.bfloat16)
    after_f = after_full.astype(jnp.float32)
    inv_rms = lax.rsqrt(jnp.mean(after_f * after_f, axis=1, keepdims=True) + norm_eps)
    normed = (after_f * inv_rms * norm_gain[None, :]).astype(jnp.bfloat16)
    after = lax.dynamic_slice_in_dim(after_full, col_first, col_count, 1)
    gate_act = jnp.dot(
        normed,
        lax.all_gather(gate_weight, "sp", axis=0, tiled=True),
        preferred_element_type=jnp.float32,
    )
    up_act = jnp.dot(
        normed,
        lax.all_gather(up_weight, "sp", axis=0, tiled=True),
        preferred_element_type=jnp.float32,
    )
    down_full = lax.all_gather(down_weight, "sp", axis=0, tiled=True)
    hidden = (jax.nn.silu(gate_act) * up_act).astype(jnp.bfloat16)
    summed = lax.psum_scatter(
        lax.dot_general(
            down_full, hidden, (((1,), (1,)), ((), ())), preferred_element_type=jnp.float32
        ).astype(jnp.bfloat16),
        "tp",
        scatter_dimension=0,
        tiled=True,
    ).astype(jnp.float32)
    return (after.astype(jnp.float32) + summed.T).astype(jnp.bfloat16)


MESH = pl.DeviceIdType.MESH
NT = (((1,), (1,)), ((), ()))


def dot(a, b, dims=(((1,), (0,)), ((), ()))):
    return lax.dot_general(a, b, dims, preferred_element_type=jnp.float32)


def when(cond, f):
    if cond is None:
        f()
    else:
        pl.when(cond)(f)


def kernel(
    S, T, W, N,
    res_hbm, q_ref, k_ref, v_ref, doc_ref, sink_ref, ow_hbm, gain_ref, g_hbm, u_hbm, d_hbm,
    out_ref,
    G, kx, vx, dx, att, res_v, ow_v, after, normed, ga, ua, hidden, dsend, drecv, ysend, yrecv, zsend, zrecv, own_sum,
    w_send, w_recv, tail_send, tail_recv, loc, ow_send, ow_recv, att_send, att_recv, n_send, n_recv,
    d_send, d_recv, y_send, y_recv, z_send, z_recv,
):
    s = lax.axis_index("sp")
    t = lax.axis_index("tp")
    R = q_ref.shape[0]
    C = gain_ref.shape[2]
    D = T * C
    K = D // S
    F = g_hbm.shape[1]
    HK = K // 2
    PER = C // K
    z, x = s // 2, s % 2
    p, c = z % 2, t % 2
    wide = p == c
    n1_z, fr_z, ot_z = z + 1 - 2 * p, (z + 2) % 4, 3 - z
    xp = z * 2 + 1 - x
    n1, fr, ot = n1_z * 2 + x, fr_z * 2 + x, ot_z * 2 + x
    n1_x, fr_x, ot_x = n1_z * 2 + 1 - x, fr_z * 2 + 1 - x, ot_z * 2 + 1 - x
    mid = (z == 1) | (z == 2)
    outer = (z == 0) | (z == 3)
    tc = t + 1 - 2 * c
    ty = (t + 2) % T

    weights = (g_hbm, u_hbm, d_hbm)
    ow_parts = [
        pltpu.make_async_copy(ow_hbm.at[:, i * C:(i + 1) * C], ow_v.at[t, i], loc.at[3 + i]) for i in range(T)
    ]
    res_parts = [
        pltpu.make_async_copy(res_hbm.at[:, i * C:(i + 1) * C], res_v.at[i], loc.at[3 + T + i]) for i in range(T)
    ]
    for cp in ow_parts + res_parts:
        cp.start()

    def split(is_wide, cond, f):
        for flag, width in ((is_wide, W), (jnp.logical_not(is_wide), N)):
            both = flag if cond is None else flag & cond
            pl.when(both)(functools.partial(f, width))

    def columns(q, width):
        return pl.ds(pl.multiple_of(q * (F - width), 128), width)

    def local(m, width):
        return pltpu.make_async_copy(
            weights[m].at[:, columns(p, width)], G.at[m, s, :, pl.ds(0, width)], loc.at[m])

    for m in range(3):
        split(wide, None, lambda width: local(m, width).start())

    barrier = pltpu.get_barrier_semaphore()
    peers = [(xp, t, None), (fr, t, None), (n1, t, None), (ot, t, mid)]
    peers += [(s, (t + d) % T, None) for d in range(1, T)]
    peers += [((s + 1) % S, t, (x == 1) & (z < 3)), ((s + S - 1) % S, t, (x == 0) & (z > 0))]
    for a, b, cond in peers:
        when(cond, lambda: pl.semaphore_signal(barrier, inc=1, device_id=(a, b), device_id_type=MESH))
    present = sum(1 if cond is None else cond.astype(jnp.int32) for _, _, cond in peers)
    pl.semaphore_wait(barrier, present)

    finish = []

    def go(cond, cp):
        when(cond, cp.start)
        finish.append(lambda: when(cond, cp.wait_send))

    def remote(src, dst, send_sem, recv_sem, to):
        return pltpu.make_async_remote_copy(
            src_ref=src, dst_ref=dst, send_sem=send_sem, recv_sem=recv_sem, device_id=to, device_id_type=MESH)

    tails = []
    for i, (a, b) in enumerate((
        (k_ref.at[pl.ds(R - WINDOW, WINDOW)], kx.at[pl.ds(0, WINDOW)]),
        (v_ref.at[pl.ds(R - WINDOW, WINDOW)], vx.at[pl.ds(0, WINDOW)]),
        (doc_ref.at[pl.ds(doc_ref.shape[0] - 8, 8)], dx.at[pl.ds(0, 8)]),
    )):
        cp = remote(a, b, tail_send.at[i], tail_recv.at[i], ((s + 1) % S, t))
        go(s < S - 1, cp)
        tails.append(cp)

    count = [0]

    def weight(kind, m, h, src=None, cond=None):
        q, to = {
            "A": (1 - p, n1), "B": (p, fr), "C": (1 - p, ot), "D": (p, fr), "X": (p, xp),
        }[kind]
        rows = pl.ds(h * HK, HK)
        sem = w_send.at[count[0]]
        count[0] += 1

        def copy(width):
            part = pl.ds(0, width)
            if src is None:
                return remote(weights[m].at[rows, columns(q, width)], G.at[m, s, rows, part],
                              sem, w_recv.at[m, s, h], (to, t))
            place = G.at[m, src, rows, part]
            return remote(place, place, sem, w_recv.at[m, src, h], (to, t))

        split(q == c, cond, lambda width: copy(width).start())
        finish.append(lambda: split(q == c, cond, lambda width: copy(width).wait_send()))

    def recv(m, src, h):
        def wait(width):
            place = G.at[m, src, pl.ds(h * HK, HK), pl.ds(0, width)]
            remote(place, place, w_send.at[0], w_recv.at[m, src, h], (xp, t)).wait_recv()
        split(wide, None, wait)

    def landed(ref, sem):
        remote(ref, ref, w_send.at[0], sem, (s, tc)).wait_recv()

    GU = ((0, 0), (1, 0), (0, 1), (1, 1))
    DN = ((2, 0), (2, 1))

    for m, h in GU:
        weight("A", m, h)
        weight("X", m, h)
    for i in range(T):
        part = ow_hbm.at[:, i * C:(i + 1) * C]
        go(None, remote(part, ow_v.at[t, i], ow_send.at[0, i], ow_recv.at[t, i], (s, ty)))
        go(None, remote(part, ow_v.at[t, i], ow_send.at[1, i], ow_recv.at[t, i], (s, tc)))
    for m, h in GU[:2]:
        weight("C", m, h, cond=mid)
        weight("B", m, h)
    weight("C", 0, 1, cond=mid)
    weight("B", 0, 1)
    weight("B", 1, 1, cond=outer)

    @pl.when(jnp.logical_not(wide))
    def _():
        def clear(i, carry):
            for m in range(3):
                G[m, i, :, N:W] = jnp.zeros((K, W - N), jnp.bfloat16)
            return carry
        if W > N:
            lax.fori_loop(0, S, clear, 0)

    @pl.when(s == 0)
    def _():
        kx[pl.ds(0, WINDOW), :] = jnp.zeros((WINDOW, kx.shape[1]), jnp.bfloat16)
        vx[pl.ds(0, WINDOW), :] = jnp.zeros((WINDOW, vx.shape[1]), jnp.bfloat16)
        dx[pl.ds(0, 8), :] = jnp.zeros((8, dx.shape[1]), jnp.int32)

    kx[pl.ds(WINDOW, R), :] = k_ref[...]
    vx[pl.ds(WINDOW, R), :] = v_ref[...]
    dx[pl.ds(8, doc_ref.shape[0]), :] = doc_ref[...]
    for cp in tails:
        when(s > 0, cp.wait_recv)
    heads = q_ref.shape[1] // HEAD_DIM

    def block(b, carry):
        rows = pl.ds(pl.multiple_of(b * WINDOW, WINDOW), WINDOW)
        band = pl.ds(pl.multiple_of(b * WINDOW, WINDOW), 2 * WINDOW)
        prev = dx[pl.ds(pl.multiple_of(b * 8, 8), 8), :][0:1].astype(jnp.float32)
        own = dx[pl.ds(pl.multiple_of(b * 8 + 8, 8), 8), :][0:1].astype(jnp.float32)
        doc_q = jnp.broadcast_to(own, (WINDOW, WINDOW)).T
        i = lax.broadcasted_iota(jnp.int32, (WINDOW, WINDOW), 0)
        j = lax.broadcasted_iota(jnp.int32, (WINDOW, WINDOW), 1)
        first = s * R + b * WINDOW - WINDOW
        see_prev = (j > i) & (doc_q == prev) & (first + j >= 0)
        see_own = (j <= i) & (doc_q == own)
        visible = jnp.concatenate(
            [see_prev.astype(jnp.float32), see_own.astype(jnp.float32)], axis=1) > 0.5
        for h in range(heads):
            kv = h // GROUP
            cols = slice(kv * HEAD_DIM, (kv + 1) * HEAD_DIM)
            q = q_ref[rows, h * HEAD_DIM:(h + 1) * HEAD_DIM]
            scores = dot(q, kx[band, cols], NT) * HEAD_DIM ** (-0.5)
            scores = jnp.where(visible, scores, neg_big)
            sink = sink_ref[h]
            row_max = jnp.maximum(scores.max(-1, keepdims=True), sink)
            expo = jnp.where(visible, jnp.exp(scores - row_max), 0.0)
            total = expo.sum(-1, keepdims=True) + jnp.exp(sink - row_max)
            w = (expo / total).astype(jnp.bfloat16)
            att[t, rows, h * HEAD_DIM:(h + 1) * HEAD_DIM] = dot(w, vx[band, cols]).astype(jnp.bfloat16)
        return carry

    lax.fori_loop(0, R // WINDOW, block, 0)

    go(None, remote(att.at[t], att.at[t], att_send.at[0], att_recv.at[t], (s, ty)))
    go(None, remote(att.at[t], att.at[t], att_send.at[1], att_recv.at[t], (s, tc)))

    def ow_relay(i):
        landed(ow_v.at[ty, i], ow_recv.at[ty, i])
        go(None, remote(ow_v.at[ty, i], ow_v.at[ty, i], ow_send.at[2, i], ow_recv.at[ty, i], (s, tc)))

    ow_relay(0)
    for i, (m, h) in enumerate(GU):
        recv(m, n1, h)
        weight("X", m, h, src=n1)
        weight("D", m, h, src=n1, cond=mid)
        if i == 1:
            weight("C", 1, 1, cond=mid)
            weight("B", 1, 1, cond=mid)
        if i < 3:
            ow_relay(i + 1)
    for m, h in DN:
        weight("X", m, h)
        weight("C", m, h, cond=mid)
        weight("B", m, h, cond=mid)

    landed(att.at[ty], att_recv.at[ty])
    go(None, remote(att.at[ty], att.at[ty], att_send.at[2], att_recv.at[ty], (s, tc)))
    for cp in ow_parts + res_parts:
        cp.wait()
    td = (tc + 2) % T
    for g in (tc, td):
        for i in range(T):
            landed(ow_v.at[g, i], ow_recv.at[g, i])
        landed(att.at[g], att_recv.at[g])

    HR = R // 2
    for r in range(2):
        rows = slice(r * HR, (r + 1) * HR)

        def project(i, square):
            total = dot(att[0, rows, :], ow_v[0, i]).astype(jnp.bfloat16).astype(jnp.float32)
            for g in range(1, T):
                total += dot(att[g, rows, :], ow_v[g, i]).astype(jnp.bfloat16).astype(jnp.float32)
            value = (res_v[i, rows, :].astype(jnp.float32) + total).astype(jnp.bfloat16)
            after[i, rows, :] = value
            value = value.astype(jnp.float32)
            return square + (value * value).sum(-1, keepdims=True)

        square = lax.fori_loop(0, T, project, jnp.zeros((HR, 1), jnp.float32))
        inv = lax.rsqrt(square / D + norm_eps)

        def norm(i, carry):
            n = (after[i, rows, :].astype(jnp.float32) * inv * gain_ref[i]).astype(jnp.bfloat16)
            for j in range(PER):
                normed[i * PER + j, rows, :] = n[:, j * K:(j + 1) * K]
            return carry

        lax.fori_loop(0, T, norm, 0)
        go(None, remote(
            normed.at[pl.ds(t * PER, PER), pl.ds(r * HR, HR)],
            normed.at[pl.ds(t * PER, PER), pl.ds(R + r * HR, HR)],
            n_send.at[0, r], n_recv.at[t, r], (n1, t)))

    for m, h in DN:
        weight("A", m, h)
        weight("B", m, h, cond=outer)

    def passed(g, r):
        return normed.at[pl.ds(g * PER, PER), pl.ds(R + r * HR, HR)]

    TM = 256

    def gate_up(src, first, last, begin=False):
        def tile(r, carry):
            rows = pl.ds(pl.multiple_of(r * TM, TM), TM)
            a = normed[src, rows, :]
            for m, acc in ((0, ga), (1, ua)):
                value = dot(a, G[m, src])
                if begin:
                    acc[rows, :] = value
                else:
                    acc[rows, :] += value
            return carry
        lax.fori_loop(first // TM, last // TM, tile, 0)

    for m in range(3):
        split(wide, None, lambda width: local(m, width).wait())
    gate_up(s, 0, R, True)
    gate_up(n1, 0, R)
    for m, h in GU:
        recv(m, fr, h)
        weight("X", m, h, src=fr)
    for m, h in GU:
        recv(m, xp, h)
    gate_up(xp, 0, R)
    for r in range(2):
        landed(passed(t, r), n_recv.at[t, r])
        go(None, remote(passed(t, r), passed(t, r), n_send.at[1, r], n_recv.at[t, r], (s, ty)))
        go(None, remote(passed(t, r), passed(t, r), n_send.at[2, r], n_recv.at[t, r], (s, tc)))
    gate_up(fr, 0, R)
    for r in range(2):
        landed(passed(ty, r), n_recv.at[ty, r])
        go(None, remote(passed(ty, r), passed(ty, r), n_send.at[3, r], n_recv.at[ty, r], (s, tc)))
    for m, h in DN:
        recv(m, n1, h)
        weight("X", m, h, src=n1)
        weight("D", m, h, src=n1, cond=mid)
    for g in (tc, td):
        for r in range(2):
            landed(passed(g, r), n_recv.at[g, r])
    gate_up(s, R, 2 * R, True)
    for src in (n1, xp, fr):
        gate_up(src, R, 2 * R)
    for m, h in GU:
        recv(m, n1_x, h)
    gate_up(n1_x, 0, 2 * R)
    for m, h in GU:
        recv(m, ot, h)
        weight("X", m, h, src=ot)
    gate_up(ot, 0, 2 * R)
    for m, h in GU:
        recv(m, fr_x, h)
    gate_up(fr_x, 0, 2 * R)
    for m, h in DN:
        recv(m, fr, h)
        weight("X", m, h, src=fr)
    for m, h in GU:
        recv(m, ot_x, h)
    gate_up(ot_x, 0, 2 * R)

    def act(r, carry):
        rows = pl.ds(pl.multiple_of(r * 32, 32), 32)
        g = ga[rows, :]
        hidden[rows, :] = (g / (1.0 + jnp.exp(-g)) * ua[rows, :]).astype(jnp.bfloat16)
        return carry

    lax.fori_loop(0, 2 * R // 32, act, 0)

    def handed(k, r):
        return remote(dsend.at[k, r], drecv.at[k, r], d_send.at[k, r], d_recv.at[k, r], (s, tc))

    def across(k, r):
        j = k % PER
        return remote(ysend.at[j, r], yrecv.at[j, r], y_send.at[j, r], y_recv.at[j, r], (s, ty))

    def back(k):
        j = k % PER
        return remote(zsend.at[j], zrecv.at[j], z_send.at[j], z_recv.at[j], (n1, t))

    def down(k):
        keep = (k // PER) % 2 == c
        for r in (1, 0):
            value = dot(hidden[r * R:(r + 1) * R, :], G[2, k], NT).astype(jnp.bfloat16)
            dsend[k, r] = value
            pl.when(jnp.logical_not(keep))(lambda: handed(k, r).start())
        finish.append(lambda: pl.when(jnp.logical_not(keep))(
            lambda: [handed(k, r).wait_send() for r in (1, 0)] and None))

    def pair(k, r):
        landed(drecv.at[k, r], d_recv.at[k, r])
        return dsend[k, r].astype(jnp.float32) + drecv[k, r].astype(jnp.float32)

    def cross(k):
        @pl.when(k // PER == ty)
        def _():
            for r in (1, 0):
                ysend[k % PER, r] = pair(k, r).astype(jnp.bfloat16)
                across(k, r).start()

    def settle(k):
        @pl.when(k // PER == t)
        def _():
            j = k % PER
            for r in (1, 0):
                total = pair(k, r)
                landed(yrecv.at[j, r], y_recv.at[j, r])
                total += yrecv[j, r].astype(jnp.float32)
                if r == 1:
                    zsend[j] = total.astype(jnp.bfloat16)
                    back(k).start()
                else:
                    own_sum[j] = total

    order = (s, n1, xp, fr, n1_x, ot, fr_x, ot_x)
    for n, k in enumerate(order):
        if n == 3:
            pass
        elif k is ot:
            for m, h in DN:
                recv(m, k, h)
                weight("X", m, h, src=k)
        elif n in (2, 4, 6, 7):
            for m, h in DN:
                recv(m, k, h)
        down(k)
        if n >= 1:
            cross(order[n - 1])
        if n >= 2:
            settle(order[n - 2])
    cross(order[-1])
    settle(order[-2])
    settle(order[-1])

    for j in range(PER):
        landed(zrecv.at[j], z_recv.at[j])
        cols = slice(j * K, (j + 1) * K)
        out_ref[:, cols] = (
            after[t, :, cols].astype(jnp.float32) + (own_sum[j] + zrecv[j].astype(jnp.float32))
        ).astype(jnp.bfloat16)

    for f in finish:
        f()
    for j in range(PER):
        back(j).wait_send()
        for r in (0, 1):
            across(j, r).wait_send()


def fused(residual, queries, keys, values, documents, sinks, out_weight, norm_gain, gate_weight, up_weight, down_weight):
    S, T = lax.axis_size("sp"), lax.axis_size("tp")
    R, D = residual.shape
    F = gate_weight.shape[1]
    C, K = D // T, D // S
    W = (F // 128 + 1) // 2 * 128
    N = F - W
    PER = C // K
    blocks = R // WINDOW
    docs = jnp.broadcast_to(documents.reshape(blocks, 1, WINDOW), (blocks, 8, WINDOW)).reshape(blocks * 8, WINDOW)
    bf, f32 = jnp.bfloat16, jnp.float32
    vm, hbm = pl.BlockSpec(memory_space=pltpu.VMEM), pl.BlockSpec(memory_space=pl.ANY)
    dma = pltpu.SemaphoreType.DMA
    scratch = [
        pltpu.VMEM((3, S, K, W), bf),
        pltpu.VMEM((R + WINDOW, keys.shape[1]), bf),
        pltpu.VMEM((R + WINDOW, keys.shape[1]), bf),
        pltpu.VMEM((blocks * 8 + 8, WINDOW), jnp.int32),
        pltpu.VMEM((T, R, queries.shape[1]), bf),
        pltpu.VMEM((T, R, C), bf),
        pltpu.VMEM((T, T, out_weight.shape[0], C), bf),
        pltpu.VMEM((T, R, C), bf),
        pltpu.VMEM((S, 2 * R, K), bf),
        pltpu.VMEM((2 * R, W), f32),
        pltpu.VMEM((2 * R, W), f32),
        pltpu.VMEM((2 * R, W), bf),
        pltpu.VMEM((S, 2, R, K), bf),
        pltpu.VMEM((S, 2, R, K), bf),
        pltpu.VMEM((PER, 2, R, K), bf),
        pltpu.VMEM((PER, 2, R, K), bf),
        pltpu.VMEM((PER, R, K), bf),
        pltpu.VMEM((PER, R, K), bf),
        pltpu.VMEM((PER, R, K), f32),
        dma((64,)), dma((3, S, 2)), dma((3,)), dma((3,)), dma((3 + 2 * T,)),
        dma((3, T)), dma((T, T)), dma((3,)), dma((T,)), dma((4, 2)), dma((T, 2)),
        dma((S, 2)), dma((S, 2)), dma((PER, 2)), dma((PER, 2)), dma((PER,)), dma((PER,)),
    ]
    return pl.pallas_call(
        functools.partial(kernel, S, T, W, N),
        out_shape=jax.ShapeDtypeStruct((R, C), bf),
        in_specs=[hbm, vm, vm, vm, vm, pl.BlockSpec(memory_space=pltpu.SMEM), hbm, vm, hbm, hbm, hbm],
        out_specs=vm,
        scratch_shapes=scratch,
        compiler_params=pltpu.CompilerParams(
            collective_id=0, has_side_effects=True, vmem_limit_bytes=60 * 2**20),
    )(residual, queries, keys, values, docs, sinks, out_weight, norm_gain.reshape(T, 1, C),
      gate_weight, up_weight, down_weight)


def line_of_four_pairs(mesh):
    return mesh.shape["sp"] == 8 and mesh.shape["tp"] == 4


def solution(mesh):
    return jax.shard_map(
        fused if line_of_four_pairs(mesh) else on_device,
        mesh=mesh,
        in_specs=(
            P("sp", None),
            P("sp", "tp"),
            P("sp", "tp"),
            P("sp", "tp"),
            P("sp"),
            P("tp"),
            P("tp", None),
            P(),
            P("sp", "tp"),
            P("sp", "tp"),
            P("sp", "tp"),
        ),
        out_specs=P("sp", "tp"),
        check_vma=False,
    )
```

time: 195 us -> 167 us (0.86)
  Pallas kernels: 190 us -> 162 us
    pallas_call x1, Pallas kernels: 190 us -> 162 us  [fused(): pl.pallas_call(functools.partial(kernel, S, T, W, N), out_shape=jax.Shape...]
where the time goes in v1:
time: 167 us; the launch traced here: 165 us
  Pallas kernels  162 us (97%)
  local copies, waits for them, and re-layouts  3.16 us (2%)
    pallas_call x1, Pallas kernels, fused(): pl.pallas_call(functools.partial(kernel, S, T, W, N), out_shape=jax.Shape...  162 us

profile of v1, /device:TPU:0, one launch (start us, length us, event | category | flops | bytes accessed | tf_op | source)
XLA Modules:
  0.0 165.1 jit_solution(4931889300011740610)
XLA Ops:
  0.0 0.0 copy-start
  0.0 0.7 copy-done
  0.7 0.6 broadcast_bitcast_fusion.doc_ref
  1.3 161.9 %shard_map.109 = bf16[512,512]{1,0:T(8,128)(2,1)} custom-call(bf16[512,2048]{1,0:T(8,128)(2,1)} %res_hbm.1, bf16[512,256]{1,0:T(8,128)(2,1)} %q_ref.1, bf16[512,128]{1,0:T(8,128)(2,1)} %k_ref.1, bf16[512,128]{1,0:T(8,128)(2,1)} %v_ref.1, s32[32,128]{1,0:T(8,128)} %broadcast_bitcast_fusion.doc_ref, f32[4]{0:T(128)} %sink_ref.1, bf16[256,2048]{1,0:T(8,128)(2,1)} %ow_hbm.1, ...), custom_call_target="tpu_custom_call" | custom-call | tf_op jit(solution)/shard_map/pallas_call | solution.py:573
  163.2 1.9 %copy.13 = bf16[512,512]{1,0:T(8,128)(2,1)} copy(bf16[512,512]{1,0:T(8,128)(2,1)} %shard_map.109) | data formatting | bytes 1048576
Async XLA Ops:
  0.0 0.7 copy-start

commit v2 on v1

--- a/solution.py
+++ b/solution.py
@@ -162,6 +162,8 @@
     n1, fr, ot = n1_z * 2 + x, fr_z * 2 + x, ot_z * 2 + x
     n1_x, fr_x, ot_x = n1_z * 2 + 1 - x, fr_z * 2 + 1 - x, ot_z * 2 + 1 - x
     mid = (z == 1) | (z == 2)
+    one, two = jnp.where(mid, fr, ot), jnp.where(mid, ot, fr)
+    one_x, two_x = jnp.where(mid, fr_x, ot_x), jnp.where(mid, ot_x, fr_x)
     outer = (z == 0) | (z == 3)
     tc = t + 1 - 2 * c
     ty = (t + 2) % T
@@ -241,11 +243,11 @@
         split(q == c, cond, lambda width: copy(width).start())
         finish.append(lambda: split(q == c, cond, lambda width: copy(width).wait_send()))
 
-    def recv(m, src, h):
+    def recv(m, src, h, cond=None):
         def wait(width):
             place = G.at[m, src, pl.ds(h * HK, HK), pl.ds(0, width)]
             remote(place, place, w_send.at[0], w_recv.at[m, src, h], (xp, t)).wait_recv()
-        split(wide, None, wait)
+        split(wide, cond, wait)
 
     def landed(ref, sem):
         remote(ref, ref, w_send.at[0], sem, (s, tc)).wait_recv()
@@ -260,12 +262,13 @@
         part = ow_hbm.at[:, i * C:(i + 1) * C]
         go(None, remote(part, ow_v.at[t, i], ow_send.at[0, i], ow_recv.at[t, i], (s, ty)))
         go(None, remote(part, ow_v.at[t, i], ow_send.at[1, i], ow_recv.at[t, i], (s, tc)))
+    for m, h in DN:
+        weight("A", m, h, cond=mid)
     for m, h in GU[:2]:
         weight("C", m, h, cond=mid)
         weight("B", m, h)
-    weight("C", 0, 1, cond=mid)
-    weight("B", 0, 1)
-    weight("B", 1, 1, cond=outer)
+    for m, h in GU[2:]:
+        weight("B", m, h, cond=outer)
 
     @pl.when(jnp.logical_not(wide))
     def _():
@@ -325,21 +328,30 @@
         landed(ow_v.at[ty, i], ow_recv.at[ty, i])
         go(None, remote(ow_v.at[ty, i], ow_v.at[ty, i], ow_send.at[2, i], ow_recv.at[ty, i], (s, tc)))
 
+    def pass_on(m, h, src, cond=None):
+        recv(m, src, h, cond)
+        weight("X", m, h, src=src, cond=cond)
+
+    pass_on(0, 0, n1)
+    weight("D", 0, 0, src=n1, cond=mid)
+    for m, h in (GU[2], GU[3], DN[0]):
+        weight("C", m, h, cond=mid)
+    pass_on(1, 0, n1)
+    weight("D", 1, 0, src=n1, cond=mid)
+    weight("B", 0, 1, cond=mid)
     ow_relay(0)
-    for i, (m, h) in enumerate(GU):
-        recv(m, n1, h)
-        weight("X", m, h, src=n1)
-        weight("D", m, h, src=n1, cond=mid)
-        if i == 1:
-            weight("C", 1, 1, cond=mid)
-            weight("B", 1, 1, cond=mid)
-        if i < 3:
-            ow_relay(i + 1)
-    for m, h in DN:
-        weight("X", m, h)
-        weight("C", m, h, cond=mid)
-        weight("B", m, h, cond=mid)
-
+    pass_on(0, 0, ot, mid)
+    pass_on(0, 0, fr, outer)
+    ow_relay(1)
+    pass_on(0, 1, n1)
+    weight("D", 0, 1, src=n1, cond=mid)
+    weight("B", 1, 1, cond=mid)
+    pass_on(1, 1, n1)
+    weight("D", 1, 1, src=n1, cond=mid)
+    ow_relay(2)
+    pass_on(1, 0, ot, mid)
+    pass_on(1, 0, fr, outer)
+    ow_relay(3)
     landed(att.at[ty], att_recv.at[ty])
     go(None, remote(att.at[ty], att.at[ty], att_send.at[2], att_recv.at[ty], (s, tc)))
     for cp in ow_parts + res_parts:
@@ -379,8 +391,7 @@
             n_send.at[0, r], n_recv.at[t, r], (n1, t)))
 
     for m, h in DN:
-        weight("A", m, h)
-        weight("B", m, h, cond=outer)
+        weight("A", m, h, cond=outer)
 
     def passed(g, r):
         return normed.at[pl.ds(g * PER, PER), pl.ds(R + r * HR, HR)]
@@ -402,45 +413,55 @@
 
     for m in range(3):
         split(wide, None, lambda width: local(m, width).wait())
+    for m, h in GU:
+        pass_on(m, h, fr, mid)
+    for m, h in DN:
+        weight("X", m, h, cond=outer)
     gate_up(s, 0, R, True)
     gate_up(n1, 0, R)
-    for m, h in GU:
-        recv(m, fr, h)
-        weight("X", m, h, src=fr)
-    for m, h in GU:
-        recv(m, xp, h)
-    gate_up(xp, 0, R)
+    pass_on(0, 0, ot, outer)
+    for src in (xp, n1_x):
+        for m, h in GU:
+            recv(m, src, h)
+        gate_up(src, 0, R)
+    pass_on(0, 1, ot, mid)
     for r in range(2):
         landed(passed(t, r), n_recv.at[t, r])
         go(None, remote(passed(t, r), passed(t, r), n_send.at[1, r], n_recv.at[t, r], (s, ty)))
         go(None, remote(passed(t, r), passed(t, r), n_send.at[2, r], n_recv.at[t, r], (s, tc)))
-    gate_up(fr, 0, R)
+    pass_on(1, 1, ot, mid)
+    for m, h in DN:
+        weight("X", m, h, cond=mid)
+    pass_on(1, 0, ot, outer)
     for r in range(2):
         landed(passed(ty, r), n_recv.at[ty, r])
         go(None, remote(passed(ty, r), passed(ty, r), n_send.at[3, r], n_recv.at[ty, r], (s, tc)))
     for m, h in DN:
-        recv(m, n1, h)
-        weight("X", m, h, src=n1)
+        recv(m, n1, h, mid)
+        weight("X", m, h, src=n1, cond=mid)
         weight("D", m, h, src=n1, cond=mid)
+        weight("B", m, h, cond=mid)
+        if h == 0:
+            weight("C", 2, 1, cond=mid)
+    pass_on(0, 1, fr, outer)
     for g in (tc, td):
         for r in range(2):
             landed(passed(g, r), n_recv.at[g, r])
     gate_up(s, R, 2 * R, True)
-    for src in (n1, xp, fr):
-        gate_up(src, R, 2 * R)
-    for m, h in GU:
-        recv(m, n1_x, h)
-    gate_up(n1_x, 0, 2 * R)
-    for m, h in GU:
-        recv(m, ot, h)
-        weight("X", m, h, src=ot)
+    gate_up(n1, R, 2 * R)
+    pass_on(0, 1, ot, outer)
+    gate_up(xp, R, 2 * R)
+    gate_up(n1_x, R, 2 * R)
+    pass_on(1, 1, fr, outer)
+    gate_up(fr, 0, 2 * R)
+    pass_on(1, 1, ot, outer)
+    for m, h in DN:
+        weight("B", m, h, cond=outer)
+        pass_on(m, h, n1, outer)
     gate_up(ot, 0, 2 * R)
     for m, h in GU:
         recv(m, fr_x, h)
     gate_up(fr_x, 0, 2 * R)
-    for m, h in DN:
-        recv(m, fr, h)
-        weight("X", m, h, src=fr)
     for m, h in GU:
         recv(m, ot_x, h)
     gate_up(ot_x, 0, 2 * R)
@@ -456,16 +477,17 @@
     def handed(k, r):
         return remote(dsend.at[k, r], drecv.at[k, r], d_send.at[k, r], d_recv.at[k, r], (s, tc))
 
-    def across(k, r):
-        j = k % PER
-        return remote(ysend.at[j, r], yrecv.at[j, r], y_send.at[j, r], y_recv.at[j, r], (s, ty))
+    def across(j):
+        return remote(ysend.at[j], yrecv.at[j], y_send.at[j], y_recv.at[j], (s, ty))
 
     def back(k):
-        j = k % PER
-        return remote(zsend.at[j], zrecv.at[j], z_send.at[j], z_recv.at[j], (n1, t))
+        return remote(zsend.at[k], zrecv.at[k], z_send.at[k], z_recv.at[k], (n1, t))
+
+    def kept(k):
+        return (k // PER) % 2 == c
 
     def down(k):
-        keep = (k // PER) % 2 == c
+        keep = kept(k)
         for r in (1, 0):
             value = dot(hidden[r * R:(r + 1) * R, :], G[2, k], NT).astype(jnp.bfloat16)
             dsend[k, r] = value
@@ -478,59 +500,78 @@
         return dsend[k, r].astype(jnp.float32) + drecv[k, r].astype(jnp.float32)
 
     def cross(k):
-        @pl.when(k // PER == ty)
+        @pl.when(kept(k))
         def _():
-            for r in (1, 0):
-                ysend[k % PER, r] = pair(k, r).astype(jnp.bfloat16)
-                across(k, r).start()
+            zsend[k] = pair(k, 1).astype(jnp.bfloat16)
+            back(k).start()
+        finish.append(lambda: pl.when(kept(k))(lambda: back(k).wait_send()))
 
     def settle(k):
-        @pl.when(k // PER == t)
+        @pl.when(kept(k))
         def _():
             j = k % PER
-            for r in (1, 0):
-                total = pair(k, r)
-                landed(yrecv.at[j, r], y_recv.at[j, r])
-                total += yrecv[j, r].astype(jnp.float32)
-                if r == 1:
-                    zsend[j] = total.astype(jnp.bfloat16)
-                    back(k).start()
-                else:
-                    own_sum[j] = total
-
-    order = (s, n1, xp, fr, n1_x, ot, fr_x, ot_x)
-    for n, k in enumerate(order):
-        if n == 3:
-            pass
-        elif k is ot:
-            for m, h in DN:
-                recv(m, k, h)
-                weight("X", m, h, src=k)
-        elif n in (2, 4, 6, 7):
-            for m, h in DN:
-                recv(m, k, h)
-        down(k)
-        if n >= 1:
-            cross(order[n - 1])
-        if n >= 2:
-            settle(order[n - 2])
-    cross(order[-1])
-    settle(order[-2])
-    settle(order[-1])
+            total = pair(k, 0)
+            landed(zrecv.at[k], z_recv.at[k])
+            total += zrecv[k].astype(jnp.float32)
+
+            @pl.when(k // PER == t)
+            def _():
+                own_sum[j] = total
+
+            @pl.when(k // PER == ty)
+            def _():
+                ysend[j] = total.astype(jnp.bfloat16)
+                across(j).start()
+
+    order = (s, n1, xp, n1_x, one, two, one_x, two_x)
+    down(order[0])
+    down(order[1])
+    cross(order[0])
+    pass_on(2, 0, ot)
+    for m, h in DN:
+        recv(m, xp, h)
+    down(order[2])
+    cross(order[1])
+    pass_on(2, 0, fr)
+    for m, h in DN:
+        recv(m, n1_x, h)
+    down(order[3])
+    cross(order[2])
+    pass_on(2, 1, one)
+    down(order[4])
+    cross(order[3])
+    pass_on(2, 1, two)
+    down(order[5])
+    cross(order[4])
+    settle(order[0])
+    settle(order[1])
+    for m, h in DN:
+        recv(m, one_x, h)
+    down(order[6])
+    cross(order[5])
+    settle(order[2])
+    settle(order[3])
+    for m, h in DN:
+        recv(m, two_x, h)
+    down(order[7])
+    cross(order[6])
+    cross(order[7])
+    settle(order[4])
+    settle(order[5])
+    settle(order[6])
+    settle(order[7])
 
     for j in range(PER):
-        landed(zrecv.at[j], z_recv.at[j])
+        landed(yrecv.at[j], y_recv.at[j])
         cols = slice(j * K, (j + 1) * K)
         out_ref[:, cols] = (
-            after[t, :, cols].astype(jnp.float32) + (own_sum[j] + zrecv[j].astype(jnp.float32))
+            after[t, :, cols].astype(jnp.float32) + (own_sum[j] + yrecv[j].astype(jnp.float32))
         ).astype(jnp.bfloat16)
 
     for f in finish:
         f()
     for j in range(PER):
-        back(j).wait_send()
-        for r in (0, 1):
-            across(j, r).wait_send()
+        across(j).wait_send()
 
 
 def fused(residual, queries, keys, values, documents, sinks, out_weight, norm_gain, gate_weight, up_weight, down_weight):
@@ -561,14 +602,14 @@
         pltpu.VMEM((2 * R, W), bf),
         pltpu.VMEM((S, 2, R, K), bf),
         pltpu.VMEM((S, 2, R, K), bf),
-        pltpu.VMEM((PER, 2, R, K), bf),
-        pltpu.VMEM((PER, 2, R, K), bf),
         pltpu.VMEM((PER, R, K), bf),
         pltpu.VMEM((PER, R, K), bf),
+        pltpu.VMEM((S, R, K), bf),
+        pltpu.VMEM((S, R, K), bf),
         pltpu.VMEM((PER, R, K), f32),
-        dma((64,)), dma((3, S, 2)), dma((3,)), dma((3,)), dma((3 + 2 * T,)),
+        dma((96,)), dma((3, S, 2)), dma((3,)), dma((3,)), dma((3 + 2 * T,)),
         dma((3, T)), dma((T, T)), dma((3,)), dma((T,)), dma((4, 2)), dma((T, 2)),
-        dma((S, 2)), dma((S, 2)), dma((PER, 2)), dma((PER, 2)), dma((PER,)), dma((PER,)),
+        dma((S, 2)), dma((S, 2)), dma((PER,)), dma((PER,)), dma((S,)), dma((S,)),
     ]
     return pl.pallas_call(
         functools.partial(kernel, S, T, W, N),

time: 167 us -> 132 us (0.79)
  Pallas kernels: 162 us -> 127 us
    pallas_call x1, Pallas kernels: 162 us -> 127 us  [fused(): pl.pallas_call(functools.partial(kernel, S, T, W, N), out_shape=jax.Shape...]
where the time goes in v2:
time: 132 us; the launch traced here: 130 us
  Pallas kernels  127 us (96%)
  local copies, waits for them, and re-layouts  3.16 us (2%)
    pallas_call x1, Pallas kernels, fused(): pl.pallas_call(functools.partial(kernel, S, T, W, N), out_shape=jax.Shape...  127 us

profile of v2, /device:TPU:0, one launch (start us, length us, event | category | flops | bytes accessed | tf_op | source)
XLA Modules:
  0.0 129.9 jit_solution(15095993130230854473)
XLA Ops:
  0.0 0.0 copy-start
  0.0 0.7 copy-done
  0.7 0.6 broadcast_bitcast_fusion.doc_ref
  1.3 126.7 %shard_map.109 = bf16[512,512]{1,0:T(8,128)(2,1)} custom-call(bf16[512,2048]{1,0:T(8,128)(2,1)} %res_hbm.1, bf16[512,256]{1,0:T(8,128)(2,1)} %q_ref.1, bf16[512,128]{1,0:T(8,128)(2,1)} %k_ref.1, bf16[512,128]{1,0:T(8,128)(2,1)} %v_ref.1, s32[32,128]{1,0:T(8,128)} %broadcast_bitcast_fusion.doc_ref, f32[4]{0:T(128)} %sink_ref.1, bf16[256,2048]{1,0:T(8,128)(2,1)} %ow_hbm.1, ...), custom_call_target="tpu_custom_call" | custom-call | tf_op jit(solution)/shard_map/pallas_call | solution.py:614
  128.0 1.9 %copy.13 = bf16[512,512]{1,0:T(8,128)(2,1)} copy(bf16[512,512]{1,0:T(8,128)(2,1)} %shard_map.109) | data formatting | bytes 1048576
Async XLA Ops:
  0.0 0.7 copy-start

commit v3 on v2

--- a/solution.py
+++ b/solution.py
@@ -139,11 +139,12 @@
 
 def kernel(
     S, T, W, N,
-    res_hbm, q_ref, k_ref, v_ref, doc_ref, sink_ref, ow_hbm, gain_ref, g_hbm, u_hbm, d_hbm,
-    out_ref,
-    G, kx, vx, dx, att, res_v, ow_v, after, normed, ga, ua, hidden, dsend, drecv, ysend, yrecv, zsend, zrecv, own_sum,
+    res_hbm, q_hbm, k_hbm, v_hbm, doc_hbm, sink_ref, ow_hbm, gain_hbm, g_hbm, u_hbm, d_hbm,
+    out_hbm,
+    q_ref, doc_ref, gain_ref, out_v,
+    G, kx, vx, dx, att, res_v, ow_v, after, normed, ga, ua, hidden, dsend, drecv, ysend, yrecv, zsend, zrecv, own_sum, nsend, nrecv,
     w_send, w_recv, tail_send, tail_recv, loc, ow_send, ow_recv, att_send, att_recv, n_send, n_recv,
-    d_send, d_recv, y_send, y_recv, z_send, z_recv,
+    d_send, d_recv, y_send, y_recv, z_send, z_recv, o_sem, o_send, o_recv,
 ):
     s = lax.axis_index("sp")
     t = lax.axis_index("tp")
@@ -175,7 +176,12 @@
     res_parts = [
         pltpu.make_async_copy(res_hbm.at[:, i * C:(i + 1) * C], res_v.at[i], loc.at[3 + T + i]) for i in range(T)
     ]
-    for cp in ow_parts + res_parts:
+    firsts = [
+        pltpu.make_async_copy(a, b, loc.at[3 + 2 * T + i]) for i, (a, b) in enumerate((
+            (doc_hbm, doc_ref), (k_hbm, kx.at[pl.ds(WINDOW, R)]), (v_hbm, vx.at[pl.ds(WINDOW, R)]),
+            (q_hbm, q_ref), (gain_hbm, gain_ref)))
+    ]
+    for cp in firsts + ow_parts + res_parts:
         cp.start()
 
     def split(is_wide, cond, f):
@@ -202,6 +208,10 @@
     present = sum(1 if cond is None else cond.astype(jnp.int32) for _, _, cond in peers)
     pl.semaphore_wait(barrier, present)
 
+    firsts[0].wait()
+    blocks = doc_ref.shape[0]
+    for i in range(blocks):
+        dx[8 + 8 * i:16 + 8 * i, :] = jnp.broadcast_to(doc_ref[i:i + 1, :], (8, WINDOW))
     finish = []
 
     def go(cond, cp):
@@ -214,9 +224,9 @@
 
     tails = []
     for i, (a, b) in enumerate((
-        (k_ref.at[pl.ds(R - WINDOW, WINDOW)], kx.at[pl.ds(0, WINDOW)]),
-        (v_ref.at[pl.ds(R - WINDOW, WINDOW)], vx.at[pl.ds(0, WINDOW)]),
-        (doc_ref.at[pl.ds(doc_ref.shape[0] - 8, 8)], dx.at[pl.ds(0, 8)]),
+        (k_hbm.at[pl.ds(R - WINDOW, WINDOW)], kx.at[pl.ds(0, WINDOW)]),
+        (v_hbm.at[pl.ds(R - WINDOW, WINDOW)], vx.at[pl.ds(0, WINDOW)]),
+        (dx.at[pl.ds(8 * blocks, 8)], dx.at[pl.ds(0, 8)]),
     )):
         cp = remote(a, b, tail_send.at[i], tail_recv.at[i], ((s + 1) % S, t))
         go(s < S - 1, cp)
@@ -285,9 +295,8 @@
         vx[pl.ds(0, WINDOW), :] = jnp.zeros((WINDOW, vx.shape[1]), jnp.bfloat16)
         dx[pl.ds(0, 8), :] = jnp.zeros((8, dx.shape[1]), jnp.int32)
 
-    kx[pl.ds(WINDOW, R), :] = k_ref[...]
-    vx[pl.ds(WINDOW, R), :] = v_ref[...]
-    dx[pl.ds(8, doc_ref.shape[0]), :] = doc_ref[...]
+    for cp in firsts[1:]:
+        cp.wait()
     for cp in tails:
         when(s > 0, cp.wait_recv)
     heads = q_ref.shape[1] // HEAD_DIM
@@ -474,104 +483,193 @@
 
     lax.fori_loop(0, 2 * R // 32, act, 0)
 
-    def handed(k, r):
-        return remote(dsend.at[k, r], drecv.at[k, r], d_send.at[k, r], d_recv.at[k, r], (s, tc))
-
-    def across(j):
-        return remote(ysend.at[j], yrecv.at[j], y_send.at[j], y_recv.at[j], (s, ty))
-
-    def back(k):
-        return remote(zsend.at[k], zrecv.at[k], z_send.at[k], z_recv.at[k], (n1, t))
+    def handed(k, h, r):
+        return remote(dsend.at[k, h, r], drecv.at[k, h, r], d_send.at[k, 2 * h + r], d_recv.at[k, 2 * h + r], (s, tc))
+
+    def across(j, h):
+        return remote(ysend.at[j, h], yrecv.at[j, h], y_send.at[j, h], y_recv.at[j, h], (s, ty))
+
+    def over(j, h):
+        return remote(nsend.at[j, h], nrecv.at[j, h], o_send.at[j, h], o_recv.at[j, h], (s, ty))
+
+    def back(k, h):
+        return remote(zsend.at[k, h], zrecv.at[k, h], z_send.at[k, h], z_recv.at[k, h], (n1, t))
+
+    def add(out, at, *terms):
+        def rows_of(i, carry):
+            rows = pl.ds(pl.multiple_of(i * WINDOW, WINDOW), WINDOW)
+            total = None
+            for ref, where in terms:
+                value = ref[(*where, rows, slice(None))].astype(jnp.float32)
+                total = value if total is None else total + value
+            out[(*at, rows, slice(None))] = total.astype(out.dtype)
+            return carry
+        lax.fori_loop(0, R // WINDOW, rows_of, 0)
 
     def kept(k):
         return (k // PER) % 2 == c
 
-    def down(k):
-        keep = kept(k)
+    def down(k, *hs):
+        given = jnp.logical_not(kept(k))
+        value = dot(hidden[...], G[2, k, hs[0] * HK:(hs[-1] + 1) * HK, :], NT).astype(jnp.bfloat16)
         for r in (1, 0):
-            value = dot(hidden[r * R:(r + 1) * R, :], G[2, k], NT).astype(jnp.bfloat16)
-            dsend[k, r] = value
-            pl.when(jnp.logical_not(keep))(lambda: handed(k, r).start())
-        finish.append(lambda: pl.when(jnp.logical_not(keep))(
-            lambda: [handed(k, r).wait_send() for r in (1, 0)] and None))
-
-    def pair(k, r):
-        landed(drecv.at[k, r], d_recv.at[k, r])
-        return dsend[k, r].astype(jnp.float32) + drecv[k, r].astype(jnp.float32)
-
-    def cross(k):
-        @pl.when(kept(k))
+            for i, h in enumerate(hs):
+                dsend[k, h, r] = value[r * R:(r + 1) * R, i * HK:(i + 1) * HK]
+
+        @pl.when(given)
         def _():
-            zsend[k] = pair(k, 1).astype(jnp.bfloat16)
-            back(k).start()
-        finish.append(lambda: pl.when(kept(k))(lambda: back(k).wait_send()))
-
-    def settle(k):
-        @pl.when(kept(k))
+            for r in (1, 0):
+                for h in hs:
+                    handed(k, h, r).start()
+
+        def sent():
+            for h in hs:
+                for r in (1, 0):
+                    handed(k, h, r).wait_send()
+        finish.append(lambda: pl.when(given)(sent))
+
+    def pair(k, h, r):
+        landed(drecv.at[k, h, r], d_recv.at[k, 2 * h + r])
+        return (dsend, (k, h, r)), (drecv, (k, h, r))
+
+    def case(k, cond, f, *hs):
+        @pl.when(cond)
         def _():
-            j = k % PER
-            total = pair(k, 0)
-            landed(zrecv.at[k], z_recv.at[k])
-            total += zrecv[k].astype(jnp.float32)
-
-            @pl.when(k // PER == t)
-            def _():
-                own_sum[j] = total
-
-            @pl.when(k // PER == ty)
-            def _():
-                ysend[j] = total.astype(jnp.bfloat16)
-                across(j).start()
-
-    order = (s, n1, xp, n1_x, one, two, one_x, two_x)
-    down(order[0])
-    down(order[1])
-    cross(order[0])
+            for h in hs:
+                f(k % PER, h)
+
+    def cross(k, *hs):
+        def straight(j, h):
+            add(zsend, (k, h), *pair(k, h, 1))
+            back(k, h).start()
+
+        def sideways(j, h):
+            add(nsend, (j, h), *pair(k, h, 1))
+            over(j, h).start()
+
+        def plain(j, h):
+            add(ysend, (j, h), *pair(k, h, 0))
+            across(j, h).start()
+
+        case(k, outer & kept(k), straight, *hs)
+        case(k, outer & (k // PER == ty), plain, *hs)
+        case(k, mid & (k // PER == ty), sideways, *hs)
+        sends = (outer & kept(k)) | (mid & (k // PER == t))
+        finish.append(lambda: case(k, sends, lambda j, h: back(k, h).wait_send(), *hs))
+        finish.append(lambda: case(k, mid & (k // PER == ty), lambda j, h: over(j, h).wait_send(), *hs))
+
+    def lift(k, *hs):
+        def up(j, h):
+            terms = pair(k, h, 1)
+            landed(nrecv.at[j, h], o_recv.at[j, h])
+            add(zsend, (k, h), *terms, (nrecv, (j, h)))
+            back(k, h).start()
+
+        case(k, mid & (k // PER == t), up, *hs)
+
+    def settle(k, *hs):
+        def own(j, h):
+            terms = pair(k, h, 0)
+            landed(zrecv.at[k, h], z_recv.at[k, h])
+            add(own_sum, (j, h), *terms, (zrecv, (k, h)))
+
+        case(k, k // PER == t, own, *hs)
+
+    def passing(k, *hs):
+        def onward(j, h):
+            terms = pair(k, h, 0)
+            landed(zrecv.at[k, h], z_recv.at[k, h])
+            add(ysend, (j, h), *terms, (zrecv, (k, h)))
+            across(j, h).start()
+
+        case(k, mid & (k // PER == ty), onward, *hs)
+
+    def halves(src, *hs):
+        for h in hs:
+            recv(2, src, h)
+
+    down(s, 0, 1)
+    down(n1, 0, 1)
+    cross(s, 0, 1)
     pass_on(2, 0, ot)
-    for m, h in DN:
-        recv(m, xp, h)
-    down(order[2])
-    cross(order[1])
+    halves(xp, 0, 1)
+    down(xp, 0, 1)
+    cross(n1, 0, 1)
     pass_on(2, 0, fr)
-    for m, h in DN:
-        recv(m, n1_x, h)
-    down(order[3])
-    cross(order[2])
+    halves(n1_x, 0, 1)
+    down(n1_x, 0, 1)
+    cross(xp, 0, 1)
+    down(ot, 0)
+    cross(n1_x, 0, 1)
+    down(fr, 0)
+    cross(ot, 0)
+    halves(ot_x, 0)
+    down(ot_x, 0)
+    cross(fr, 0)
+    lift(s, 0, 1)
+    lift(n1, 0, 1)
     pass_on(2, 1, one)
-    down(order[4])
-    cross(order[3])
+    down(one, 1)
+    cross(ot_x, 0)
+    lift(xp, 0, 1)
+    lift(n1_x, 0, 1)
     pass_on(2, 1, two)
-    down(order[5])
-    cross(order[4])
-    settle(order[0])
-    settle(order[1])
-    for m, h in DN:
-        recv(m, one_x, h)
-    down(order[6])
-    cross(order[5])
-    settle(order[2])
-    settle(order[3])
-    for m, h in DN:
-        recv(m, two_x, h)
-    down(order[7])
-    cross(order[6])
-    cross(order[7])
-    settle(order[4])
-    settle(order[5])
-    settle(order[6])
-    settle(order[7])
-
-    for j in range(PER):
-        landed(yrecv.at[j], y_recv.at[j])
-        cols = slice(j * K, (j + 1) * K)
-        out_ref[:, cols] = (
-            after[t, :, cols].astype(jnp.float32) + (own_sum[j] + yrecv[j].astype(jnp.float32))
-        ).astype(jnp.bfloat16)
+    halves(fr_x, 0)
+    down(fr_x, 0)
+    cross(one, 1)
+    passing(s, 0, 1)
+    passing(n1, 0, 1)
+    down(two, 1)
+    cross(fr_x, 0)
+    cross(two, 1)
+    halves(one_x, 1)
+    down(one_x, 1)
+    lift(ot, 0)
+    lift(fr, 0)
+    cross(one_x, 1)
+    halves(two_x, 1)
+    down(two_x, 1)
+    passing(xp, 0, 1)
+    passing(n1_x, 0, 1)
+    cross(two_x, 1)
+    lift(ot_x, 0)
+    lift(one, 1)
+    passing(ot, 0)
+    passing(fr, 0)
+    passing(ot_x, 0)
+    lift(fr_x, 0)
+    lift(two, 1)
+    passing(one, 1)
+    passing(fr_x, 0)
+    passing(two, 1)
+    lift(one_x, 1)
+    lift(two_x, 1)
+    passing(one_x, 1)
+    passing(two_x, 1)
+    for k in (s, n1, xp, n1_x):
+        settle(k, 0, 1)
+    for k, h in ((ot, 0), (fr, 0), (ot_x, 0), (one, 1), (fr_x, 0), (two, 1), (one_x, 1), (two_x, 1)):
+        settle(k, h)
+
+    stores = []
+    for h in (0, 1):
+        for j in range(PER):
+            landed(yrecv.at[j, h], y_recv.at[j, h])
+            cols = slice((j * 2 + h) * HK, (j * 2 + h + 1) * HK)
+            out_v[:, cols] = (
+                after[t, :, cols].astype(jnp.float32) + (own_sum[j, h] + yrecv[j, h].astype(jnp.float32))
+            ).astype(jnp.bfloat16)
+            cp = pltpu.make_async_copy(out_v.at[:, cols], out_hbm.at[:, cols], o_sem.at[j, h])
+            cp.start()
+            stores.append(cp)
 
     for f in finish:
         f()
     for j in range(PER):
-        across(j).wait_send()
+        for h in (0, 1):
+            across(j, h).wait_send()
+    for cp in stores:
+        cp.wait()
 
 
 def fused(residual, queries, keys, values, documents, sinks, out_weight, norm_gain, gate_weight, up_weight, down_weight):
@@ -583,11 +681,15 @@
     N = F - W
     PER = C // K
     blocks = R // WINDOW
-    docs = jnp.broadcast_to(documents.reshape(blocks, 1, WINDOW), (blocks, 8, WINDOW)).reshape(blocks * 8, WINDOW)
+    HK = K // 2
     bf, f32 = jnp.bfloat16, jnp.float32
-    vm, hbm = pl.BlockSpec(memory_space=pltpu.VMEM), pl.BlockSpec(memory_space=pl.ANY)
+    hbm = pl.BlockSpec(memory_space=pl.ANY)
     dma = pltpu.SemaphoreType.DMA
     scratch = [
+        pltpu.VMEM((R, queries.shape[1]), bf),
+        pltpu.VMEM((blocks, WINDOW), jnp.int32),
+        pltpu.VMEM((T, 1, C), f32),
+        pltpu.VMEM((R, C), bf),
         pltpu.VMEM((3, S, K, W), bf),
         pltpu.VMEM((R + WINDOW, keys.shape[1]), bf),
         pltpu.VMEM((R + WINDOW, keys.shape[1]), bf),
@@ -600,26 +702,28 @@
         pltpu.VMEM((2 * R, W), f32),
         pltpu.VMEM((2 * R, W), f32),
         pltpu.VMEM((2 * R, W), bf),
-        pltpu.VMEM((S, 2, R, K), bf),
-        pltpu.VMEM((S, 2, R, K), bf),
-        pltpu.VMEM((PER, R, K), bf),
-        pltpu.VMEM((PER, R, K), bf),
-        pltpu.VMEM((S, R, K), bf),
-        pltpu.VMEM((S, R, K), bf),
-        pltpu.VMEM((PER, R, K), f32),
-        dma((96,)), dma((3, S, 2)), dma((3,)), dma((3,)), dma((3 + 2 * T,)),
+        pltpu.VMEM((S, 2, 2, R, HK), bf),
+        pltpu.VMEM((S, 2, 2, R, HK), bf),
+        pltpu.VMEM((PER, 2, R, HK), bf),
+        pltpu.VMEM((PER, 2, R, HK), bf),
+        pltpu.VMEM((S, 2, R, HK), bf),
+        pltpu.VMEM((S, 2, R, HK), bf),
+        pltpu.VMEM((PER, 2, R, HK), f32),
+        pltpu.VMEM((PER, 2, R, HK), bf),
+        pltpu.VMEM((PER, 2, R, HK), bf),
+        dma((96,)), dma((3, S, 2)), dma((3,)), dma((3,)), dma((8 + 2 * T,)),
         dma((3, T)), dma((T, T)), dma((3,)), dma((T,)), dma((4, 2)), dma((T, 2)),
-        dma((S, 2)), dma((S, 2)), dma((PER,)), dma((PER,)), dma((S,)), dma((S,)),
+        dma((S, 4)), dma((S, 4)), dma((PER, 2)), dma((PER, 2)), dma((S, 2)), dma((S, 2)), dma((PER, 2)), dma((PER, 2)), dma((PER, 2)),
     ]
     return pl.pallas_call(
         functools.partial(kernel, S, T, W, N),
         out_shape=jax.ShapeDtypeStruct((R, C), bf),
-        in_specs=[hbm, vm, vm, vm, vm, pl.BlockSpec(memory_space=pltpu.SMEM), hbm, vm, hbm, hbm, hbm],
-        out_specs=vm,
+        in_specs=[hbm] * 5 + [pl.BlockSpec(memory_space=pltpu.SMEM)] + [hbm] * 5,
+        out_specs=hbm,
         scratch_shapes=scratch,
         compiler_params=pltpu.CompilerParams(
             collective_id=0, has_side_effects=True, vmem_limit_bytes=60 * 2**20),
-    )(residual, queries, keys, values, docs, sinks, out_weight, norm_gain.reshape(T, 1, C),
+    )(residual, queries, keys, values, documents.reshape(blocks, WINDOW), sinks, out_weight, norm_gain.reshape(T, 1, C),
       gate_weight, up_weight, down_weight)
 
 

time: 132 us -> 125 us (0.947)
  the two profiles are of different devices: /device:TPU:0 before, /device:TPU:16 now
where the time goes in v3:
time: 125 us
  Pallas kernels  123 us (98%)
  local copies, waits for them, and re-layouts  1.87 us (1%)
    pallas_call x1, Pallas kernels, fused(): pl.pallas_call(functools.partial(kernel, S, T, W, N), out_shape=jax.Shape...  123 us

profile of v3, /device:TPU:16, one launch (start us, length us, event | category | flops | bytes accessed | tf_op | source)
XLA Modules:
  0.0 124.5 jit_solution(15070530093498687586)
XLA Ops:
  0.0 122.6 %shard_map.109 = bf16[512,512]{1,0:T(8,128)(2,1)} custom-call(bf16[512,2048]{1,0:T(8,128)(2,1)} %res_hbm.1, bf16[512,256]{1,0:T(8,128)(2,1)} %q_hbm.1, bf16[512,128]{1,0:T(8,128)(2,1)} %k_hbm.1, bf16[512,128]{1,0:T(8,128)(2,1)} %v_hbm.1, s32[4,128]{1,0:T(4,128)} %bitcast.3, f32[4]{0:T(128)} %sink_ref.1, bf16[256,2048]{1,0:T(8,128)(2,1)} %ow_hbm.1, ...), custom_call_target="tpu_custom_call" | custom-call | tf_op jit(solution)/shard_map/pallas_call | solution.py:718
  122.6 1.9 %copy.13 = bf16[512,512]{1,0:T(8,128)(2,1)} copy(bf16[512,512]{1,0:T(8,128)(2,1)} %shard_map.109) | data formatting | bytes 1048576

commit v4 on v3

--- a/solution.py
+++ b/solution.py
@@ -171,13 +171,13 @@
 
     weights = (g_hbm, u_hbm, d_hbm)
     ow_parts = [
-        pltpu.make_async_copy(ow_hbm.at[:, i * C:(i + 1) * C], ow_v.at[t, i], loc.at[3 + i]) for i in range(T)
+        pltpu.make_async_copy(ow_hbm.at[:, i * C:(i + 1) * C], ow_v.at[t, i], loc.at[0]) for i in range(T)
     ]
     res_parts = [
-        pltpu.make_async_copy(res_hbm.at[:, i * C:(i + 1) * C], res_v.at[i], loc.at[3 + T + i]) for i in range(T)
+        pltpu.make_async_copy(res_hbm.at[:, i * C:(i + 1) * C], res_v.at[i], loc.at[1]) for i in range(T)
     ]
     firsts = [
-        pltpu.make_async_copy(a, b, loc.at[3 + 2 * T + i]) for i, (a, b) in enumerate((
+        pltpu.make_async_copy(a, b, loc.at[3 + i]) for i, (a, b) in enumerate((
             (doc_hbm, doc_ref), (k_hbm, kx.at[pl.ds(WINDOW, R)]), (v_hbm, vx.at[pl.ds(WINDOW, R)]),
             (q_hbm, q_ref), (gain_hbm, gain_ref)))
     ]
@@ -194,7 +194,7 @@
 
     def local(m, width):
         return pltpu.make_async_copy(
-            weights[m].at[:, columns(p, width)], G.at[m, s, :, pl.ds(0, width)], loc.at[m])
+            weights[m].at[:, columns(p, width)], G.at[m, s, :, pl.ds(0, width)], loc.at[2])
 
     for m in range(3):
         split(wide, None, lambda width: local(m, width).start())
@@ -217,6 +217,9 @@
     def go(cond, cp):
         when(cond, cp.start)
         finish.append(lambda: when(cond, cp.wait_send))
+
+    def start(cp):
+        cp.start()
 
     def remote(src, dst, send_sem, recv_sem, to):
         return pltpu.make_async_remote_copy(
@@ -232,15 +235,12 @@
         go(s < S - 1, cp)
         tails.append(cp)
 
-    count = [0]
+    kinds = {"A": (1 - p, n1), "B": (p, fr), "C": (1 - p, ot), "D": (p, fr), "X": (p, xp)}
 
     def weight(kind, m, h, src=None, cond=None):
-        q, to = {
-            "A": (1 - p, n1), "B": (p, fr), "C": (1 - p, ot), "D": (p, fr), "X": (p, xp),
-        }[kind]
+        q, to = kinds[kind]
         rows = pl.ds(h * HK, HK)
-        sem = w_send.at[count[0]]
-        count[0] += 1
+        sem = w_send.at["ABCDX".index(kind)]
 
         def copy(width):
             part = pl.ds(0, width)
@@ -251,7 +251,15 @@
             return remote(place, place, sem, w_recv.at[m, src, h], (to, t))
 
         split(q == c, cond, lambda width: copy(width).start())
-        finish.append(lambda: split(q == c, cond, lambda width: copy(width).wait_send()))
+
+    def weights_sent(kind, sources, cond=None):
+        q, to = kinds[kind]
+
+        def wait(width):
+            place = G.at[:, pl.ds(0, sources), :, pl.ds(0, width)]
+            remote(place, place, w_send.at["ABCDX".index(kind)], w_recv.at[0, 0, 0], (to, t)).wait_send()
+
+        split(q == c, cond, wait)
 
     def recv(m, src, h, cond=None):
         def wait(width):
@@ -270,12 +278,11 @@
         weight("X", m, h)
     for i in range(T):
         part = ow_hbm.at[:, i * C:(i + 1) * C]
-        go(None, remote(part, ow_v.at[t, i], ow_send.at[0, i], ow_recv.at[t, i], (s, ty)))
-        go(None, remote(part, ow_v.at[t, i], ow_send.at[1, i], ow_recv.at[t, i], (s, tc)))
-    for m, h in DN:
-        weight("A", m, h, cond=mid)
+        start(remote(part, ow_v.at[t, i], ow_send.at[0], ow_recv.at[i], (s, ty)))
+        start(remote(part, ow_v.at[t, i], ow_send.at[1], ow_recv.at[T], (s, tc)))
+    weight("A", 2, 0, cond=mid)
+    weight("C", 0, 0, cond=mid)
     for m, h in GU[:2]:
-        weight("C", m, h, cond=mid)
         weight("B", m, h)
     for m, h in GU[2:]:
         weight("B", m, h, cond=outer)
@@ -334,8 +341,8 @@
     go(None, remote(att.at[t], att.at[t], att_send.at[1], att_recv.at[t], (s, tc)))
 
     def ow_relay(i):
-        landed(ow_v.at[ty, i], ow_recv.at[ty, i])
-        go(None, remote(ow_v.at[ty, i], ow_v.at[ty, i], ow_send.at[2, i], ow_recv.at[ty, i], (s, tc)))
+        landed(ow_v.at[ty, i], ow_recv.at[i])
+        start(remote(ow_v.at[ty, i], ow_v.at[ty, i], ow_send.at[2], ow_recv.at[T + 1], (s, tc)))
 
     def pass_on(m, h, src, cond=None):
         recv(m, src, h, cond)
@@ -343,13 +350,12 @@
 
     pass_on(0, 0, n1)
     weight("D", 0, 0, src=n1, cond=mid)
-    for m, h in (GU[2], GU[3], DN[0]):
-        weight("C", m, h, cond=mid)
     pass_on(1, 0, n1)
     weight("D", 1, 0, src=n1, cond=mid)
+    for m, h in GU[1:]:
+        weight("C", m, h, cond=mid)
     weight("B", 0, 1, cond=mid)
     ow_relay(0)
-    pass_on(0, 0, ot, mid)
     pass_on(0, 0, fr, outer)
     ow_relay(1)
     pass_on(0, 1, n1)
@@ -357,18 +363,19 @@
     weight("B", 1, 1, cond=mid)
     pass_on(1, 1, n1)
     weight("D", 1, 1, src=n1, cond=mid)
+    weight("C", 2, 0, cond=mid)
     ow_relay(2)
-    pass_on(1, 0, ot, mid)
+    pass_on(0, 0, ot, mid)
     pass_on(1, 0, fr, outer)
     ow_relay(3)
+    pass_on(0, 0, ot, outer)
     landed(att.at[ty], att_recv.at[ty])
     go(None, remote(att.at[ty], att.at[ty], att_send.at[2], att_recv.at[ty], (s, tc)))
-    for cp in ow_parts + res_parts:
-        cp.wait()
+    pltpu.make_async_copy(ow_v.at[t], ow_v.at[t], loc.at[0]).wait()
+    pltpu.make_async_copy(res_v, res_v, loc.at[1]).wait()
     td = (tc + 2) % T
-    for g in (tc, td):
-        for i in range(T):
-            landed(ow_v.at[g, i], ow_recv.at[g, i])
+    for i, g in enumerate((tc, td)):
+        landed(ow_v.at[g], ow_recv.at[T + i])
         landed(att.at[g], att_recv.at[g])
 
     HR = R // 2
@@ -399,8 +406,8 @@
             normed.at[pl.ds(t * PER, PER), pl.ds(R + r * HR, HR)],
             n_send.at[0, r], n_recv.at[t, r], (n1, t)))
 
-    for m, h in DN:
-        weight("A", m, h, cond=outer)
+    weight("A", 2, 0, cond=outer)
+    weight("A", 2, 1)
 
     def passed(g, r):
         return normed.at[pl.ds(g * PER, PER), pl.ds(R + r * HR, HR)]
@@ -420,28 +427,31 @@
             return carry
         lax.fori_loop(first // TM, last // TM, tile, 0)
 
-    for m in range(3):
-        split(wide, None, lambda width: local(m, width).wait())
+    def local_done(width):
+        place = G.at[:, s, :, pl.ds(0, width)]
+        pltpu.make_async_copy(place, place, loc.at[2]).wait()
+
+    split(wide, None, local_done)
     for m, h in GU:
         pass_on(m, h, fr, mid)
-    for m, h in DN:
-        weight("X", m, h, cond=outer)
     gate_up(s, 0, R, True)
     gate_up(n1, 0, R)
-    pass_on(0, 0, ot, outer)
+    pass_on(1, 0, ot, outer)
+    weight("X", 2, 0, cond=outer)
     for src in (xp, n1_x):
         for m, h in GU:
             recv(m, src, h)
         gate_up(src, 0, R)
-    pass_on(0, 1, ot, mid)
+    pass_on(1, 0, ot, mid)
     for r in range(2):
         landed(passed(t, r), n_recv.at[t, r])
         go(None, remote(passed(t, r), passed(t, r), n_send.at[1, r], n_recv.at[t, r], (s, ty)))
         go(None, remote(passed(t, r), passed(t, r), n_send.at[2, r], n_recv.at[t, r], (s, tc)))
+    pass_on(0, 1, ot, mid)
     pass_on(1, 1, ot, mid)
     for m, h in DN:
         weight("X", m, h, cond=mid)
-    pass_on(1, 0, ot, outer)
+    pass_on(0, 1, fr, outer)
     for r in range(2):
         landed(passed(ty, r), n_recv.at[ty, r])
         go(None, remote(passed(ty, r), passed(ty, r), n_send.at[3, r], n_recv.at[ty, r], (s, tc)))
@@ -449,30 +459,31 @@
         recv(m, n1, h, mid)
         weight("X", m, h, src=n1, cond=mid)
         weight("D", m, h, src=n1, cond=mid)
+        if h == 1:
+            weight("C", m, h, cond=mid)
         weight("B", m, h, cond=mid)
-        if h == 0:
-            weight("C", 2, 1, cond=mid)
-    pass_on(0, 1, fr, outer)
+    pass_on(0, 1, ot, outer)
     for g in (tc, td):
         for r in range(2):
             landed(passed(g, r), n_recv.at[g, r])
     gate_up(s, R, 2 * R, True)
     gate_up(n1, R, 2 * R)
-    pass_on(0, 1, ot, outer)
+    pass_on(1, 1, fr, outer)
     gate_up(xp, R, 2 * R)
     gate_up(n1_x, R, 2 * R)
-    pass_on(1, 1, fr, outer)
-    gate_up(fr, 0, 2 * R)
     pass_on(1, 1, ot, outer)
+    weight("X", 2, 1, cond=outer)
     for m, h in DN:
         weight("B", m, h, cond=outer)
-        pass_on(m, h, n1, outer)
+    pass_on(2, 0, n1, outer)
+    gate_up(fr, 0, 2 * R)
     gate_up(ot, 0, 2 * R)
     for m, h in GU:
         recv(m, fr_x, h)
     gate_up(fr_x, 0, 2 * R)
     for m, h in GU:
         recv(m, ot_x, h)
+    pass_on(2, 1, n1, outer)
     gate_up(ot_x, 0, 2 * R)
 
     def act(r, carry):
@@ -483,8 +494,11 @@
 
     lax.fori_loop(0, 2 * R // 32, act, 0)
 
-    def handed(k, h, r):
-        return remote(dsend.at[k, h, r], drecv.at[k, h, r], d_send.at[k, 2 * h + r], d_recv.at[k, 2 * h + r], (s, tc))
+    def slot(k):
+        return k // PER // 2 * PER + k % PER
+
+    def handed(k, h):
+        return remote(dsend.at[k, h], drecv.at[k, h], d_send.at[slot(k), h], d_recv.at[slot(k), h], (s, tc))
 
     def across(j, h):
         return remote(ysend.at[j, h], yrecv.at[j, h], y_send.at[j, h], y_recv.at[j, h], (s, ty))
@@ -493,7 +507,7 @@
         return remote(nsend.at[j, h], nrecv.at[j, h], o_send.at[j, h], o_recv.at[j, h], (s, ty))
 
     def back(k, h):
-        return remote(zsend.at[k, h], zrecv.at[k, h], z_send.at[k, h], z_recv.at[k, h], (n1, t))
+        return remote(zsend.at[k, h], zrecv.at[k, h], z_send.at[slot(k), h], z_recv.at[slot(k), h], (n1, t))
 
     def add(out, at, *terms):
         def rows_of(i, carry):
@@ -518,71 +532,67 @@
 
         @pl.when(given)
         def _():
-            for r in (1, 0):
-                for h in hs:
-                    handed(k, h, r).start()
-
-        def sent():
             for h in hs:
-                for r in (1, 0):
-                    handed(k, h, r).wait_send()
-        finish.append(lambda: pl.when(given)(sent))
+                handed(k, h).start()
+
+        for h in hs:
+            finish.append(functools.partial(when, given, handed(k, h).wait_send))
 
     def pair(k, h, r):
-        landed(drecv.at[k, h, r], d_recv.at[k, 2 * h + r])
         return (dsend, (k, h, r)), (drecv, (k, h, r))
 
-    def case(k, cond, f, *hs):
-        @pl.when(cond)
+    def cross(k, *hs):
+        owned, passed_to = k // PER == t, k // PER == ty
+        for h in hs:
+            j = k % PER
+
+            @pl.when(kept(k))
+            def _():
+                landed(drecv.at[k, h], d_recv.at[slot(k), h])
+
+            if h == 0:
+                @pl.when(passed_to)
+                def _():
+                    add(nsend, (j, h), *pair(k, h, 1))
+                    over(j, h).start()
+                    add(ysend, (j, h), *pair(k, h, 0))
+                    across(j, h).start()
+                finish.append(functools.partial(when, passed_to, over(j, h).wait_send))
+                finish.append(functools.partial(when, owned, back(k, h).wait_send))
+            else:
+                @pl.when(kept(k))
+                def _():
+                    add(zsend, (k, h), *pair(k, h, 1))
+                    back(k, h).start()
+                finish.append(functools.partial(when, kept(k), back(k, h).wait_send))
+
+    def lift(k):
+        j = k % PER
+
+        @pl.when(k // PER == t)
         def _():
-            for h in hs:
-                f(k % PER, h)
-
-    def cross(k, *hs):
-        def straight(j, h):
-            add(zsend, (k, h), *pair(k, h, 1))
-            back(k, h).start()
-
-        def sideways(j, h):
-            add(nsend, (j, h), *pair(k, h, 1))
-            over(j, h).start()
-
-        def plain(j, h):
-            add(ysend, (j, h), *pair(k, h, 0))
-            across(j, h).start()
-
-        case(k, outer & kept(k), straight, *hs)
-        case(k, outer & (k // PER == ty), plain, *hs)
-        case(k, mid & (k // PER == ty), sideways, *hs)
-        sends = (outer & kept(k)) | (mid & (k // PER == t))
-        finish.append(lambda: case(k, sends, lambda j, h: back(k, h).wait_send(), *hs))
-        finish.append(lambda: case(k, mid & (k // PER == ty), lambda j, h: over(j, h).wait_send(), *hs))
-
-    def lift(k, *hs):
-        def up(j, h):
-            terms = pair(k, h, 1)
-            landed(nrecv.at[j, h], o_recv.at[j, h])
-            add(zsend, (k, h), *terms, (nrecv, (j, h)))
-            back(k, h).start()
-
-        case(k, mid & (k // PER == t), up, *hs)
+            terms = pair(k, 0, 1)
+            landed(nrecv.at[j, 0], o_recv.at[j, 0])
+            add(zsend, (k, 0), *terms, (nrecv, (j, 0)))
+            back(k, 0).start()
 
     def settle(k, *hs):
-        def own(j, h):
-            terms = pair(k, h, 0)
-            landed(zrecv.at[k, h], z_recv.at[k, h])
-            add(own_sum, (j, h), *terms, (zrecv, (k, h)))
-
-        case(k, k // PER == t, own, *hs)
-
-    def passing(k, *hs):
-        def onward(j, h):
-            terms = pair(k, h, 0)
-            landed(zrecv.at[k, h], z_recv.at[k, h])
-            add(ysend, (j, h), *terms, (zrecv, (k, h)))
-            across(j, h).start()
-
-        case(k, mid & (k // PER == ty), onward, *hs)
+        for h in hs:
+            @pl.when(k // PER == t)
+            def _():
+                terms = pair(k, h, 0)
+                landed(zrecv.at[k, h], z_recv.at[slot(k), h])
+                add(own_sum, (k % PER, h), *terms, (zrecv, (k, h)))
+
+    def passing(k):
+        j = k % PER
+
+        @pl.when(k // PER == ty)
+        def _():
+            terms = pair(k, 1, 0)
+            landed(zrecv.at[k, 1], z_recv.at[slot(k), 1])
+            add(ysend, (j, 1), *terms, (zrecv, (k, 1)))
+            across(j, 1).start()
 
     def halves(src, *hs):
         for h in hs:
@@ -606,52 +616,43 @@
     halves(ot_x, 0)
     down(ot_x, 0)
     cross(fr, 0)
-    lift(s, 0, 1)
-    lift(n1, 0, 1)
+    lift(s)
+    lift(n1)
     pass_on(2, 1, one)
     down(one, 1)
     cross(ot_x, 0)
-    lift(xp, 0, 1)
-    lift(n1_x, 0, 1)
+    lift(xp)
     pass_on(2, 1, two)
     halves(fr_x, 0)
     down(fr_x, 0)
     cross(one, 1)
-    passing(s, 0, 1)
-    passing(n1, 0, 1)
+    lift(n1_x)
+    passing(s)
+    passing(n1)
     down(two, 1)
     cross(fr_x, 0)
     cross(two, 1)
+    lift(ot)
     halves(one_x, 1)
     down(one_x, 1)
-    lift(ot, 0)
-    lift(fr, 0)
     cross(one_x, 1)
+    lift(fr)
+    passing(xp)
+    passing(n1_x)
     halves(two_x, 1)
     down(two_x, 1)
-    passing(xp, 0, 1)
-    passing(n1_x, 0, 1)
     cross(two_x, 1)
-    lift(ot_x, 0)
-    lift(one, 1)
-    passing(ot, 0)
-    passing(fr, 0)
-    passing(ot_x, 0)
-    lift(fr_x, 0)
-    lift(two, 1)
-    passing(one, 1)
-    passing(fr_x, 0)
-    passing(two, 1)
-    lift(one_x, 1)
-    lift(two_x, 1)
-    passing(one_x, 1)
-    passing(two_x, 1)
+    lift(ot_x)
+    lift(fr_x)
+    passing(one)
+    passing(two)
+    passing(one_x)
+    passing(two_x)
     for k in (s, n1, xp, n1_x):
         settle(k, 0, 1)
     for k, h in ((ot, 0), (fr, 0), (ot_x, 0), (one, 1), (fr_x, 0), (two, 1), (one_x, 1), (two_x, 1)):
         settle(k, h)
 
-    stores = []
     for h in (0, 1):
         for j in range(PER):
             landed(yrecv.at[j, h], y_recv.at[j, h])
@@ -659,17 +660,22 @@
             out_v[:, cols] = (
                 after[t, :, cols].astype(jnp.float32) + (own_sum[j, h] + yrecv[j, h].astype(jnp.float32))
             ).astype(jnp.bfloat16)
-            cp = pltpu.make_async_copy(out_v.at[:, cols], out_hbm.at[:, cols], o_sem.at[j, h])
+            cp = pltpu.make_async_copy(out_v.at[:, cols], out_hbm.at[:, cols], o_sem.at[0])
             cp.start()
-            stores.append(cp)
-
+
+    weights_sent("A", 1)
+    weights_sent("B", 1)
+    weights_sent("C", 1, mid)
+    weights_sent("D", 1, mid)
+    weights_sent("X", 4)
+    for i, to in enumerate((ty, tc, tc)):
+        remote(ow_v.at[0], ow_v.at[0], ow_send.at[i], ow_recv.at[0], (s, to)).wait_send()
     for f in finish:
         f()
     for j in range(PER):
         for h in (0, 1):
             across(j, h).wait_send()
-    for cp in stores:
-        cp.wait()
+    pltpu.make_async_copy(out_v, out_hbm, o_sem.at[0]).wait()
 
 
 def fused(residual, queries, keys, values, documents, sinks, out_weight, norm_gain, gate_weight, up_weight, down_weight):
@@ -711,9 +717,10 @@
         pltpu.VMEM((PER, 2, R, HK), f32),
         pltpu.VMEM((PER, 2, R, HK), bf),
         pltpu.VMEM((PER, 2, R, HK), bf),
-        dma((96,)), dma((3, S, 2)), dma((3,)), dma((3,)), dma((8 + 2 * T,)),
-        dma((3, T)), dma((T, T)), dma((3,)), dma((T,)), dma((4, 2)), dma((T, 2)),
-        dma((S, 4)), dma((S, 4)), dma((PER, 2)), dma((PER, 2)), dma((S, 2)), dma((S, 2)), dma((PER, 2)), dma((PER, 2)), dma((PER, 2)),
+        dma((5,)), dma((3, S, 2)), dma((3,)), dma((3,)), dma((8,)),
+        dma((3,)), dma((T + 2,)), dma((3,)), dma((T,)), dma((4, 2)), dma((T, 2)),
+        dma((S // 2, 2)), dma((S // 2, 2)), dma((PER, 2)), dma((PER, 2)), dma((S // 2, 2)), dma((S // 2, 2)),
+        dma((1,)), dma((PER, 2)), dma((PER, 2)),
     ]
     return pl.pallas_call(
         functools.partial(kernel, S, T, W, N),

time: 125 us -> 120 us (0.960)
  the two profiles are of different devices: /device:TPU:16 before, /device:TPU:0 now
where the time goes in v4:
time: 120 us; the launch traced here: 119 us
  Pallas kernels  117 us (98%)
  local copies, waits for them, and re-layouts  1.87 us (2%)
    pallas_call x1, Pallas kernels, fused(): pl.pallas_call(functools.partial(kernel, S, T, W, N), out_shape=jax.Shape...  117 us

profile of v4, /device:TPU:0, one launch (start us, length us, event | category | flops | bytes accessed | tf_op | source)
XLA Modules:
  0.0 119.3 jit_solution(1439363624600794424)
XLA Ops:
  0.0 117.4 %shard_map.109 = bf16[512,512]{1,0:T(8,128)(2,1)} custom-call(bf16[512,2048]{1,0:T(8,128)(2,1)} %res_hbm.1, bf16[512,256]{1,0:T(8,128)(2,1)} %q_hbm.1, bf16[512,128]{1,0:T(8,128)(2,1)} %k_hbm.1, bf16[512,128]{1,0:T(8,128)(2,1)} %v_hbm.1, s32[4,128]{1,0:T(4,128)} %bitcast.3, f32[4]{0:T(128)} %sink_ref.1, bf16[256,2048]{1,0:T(8,128)(2,1)} %ow_hbm.1, ...), custom_call_target="tpu_custom_call" | custom-call | tf_op jit(solution)/shard_map/pallas_call | solution.py:725
  117.4 1.9 %copy.13 = bf16[512,512]{1,0:T(8,128)(2,1)} copy(bf16[512,512]{1,0:T(8,128)(2,1)} %shard_map.109) | data formatting | bytes 1048576

commit v5 on v4

--- a/solution.py
+++ b/solution.py
@@ -140,11 +140,11 @@
 def kernel(
     S, T, W, N,
     res_hbm, q_hbm, k_hbm, v_hbm, doc_hbm, sink_ref, ow_hbm, gain_hbm, g_hbm, u_hbm, d_hbm,
-    out_hbm,
-    q_ref, doc_ref, gain_ref, out_v,
+    out_ref,
+    q_ref, doc_ref, gain_ref,
     G, kx, vx, dx, att, res_v, ow_v, after, normed, ga, ua, hidden, dsend, drecv, ysend, yrecv, zsend, zrecv, own_sum, nsend, nrecv,
-    w_send, w_recv, tail_send, tail_recv, loc, ow_send, ow_recv, att_send, att_recv, n_send, n_recv,
-    d_send, d_recv, y_send, y_recv, z_send, z_recv, o_sem, o_send, o_recv,
+    w_send, w_recv, last_recv, tail_send, tail_recv, loc, ow_send, ow_recv, att_send, att_recv, n_send, n_recv,
+    d_send, d_recv, y_send, y_recv, z_send, z_recv, o_send, o_recv,
 ):
     s = lax.axis_index("sp")
     t = lax.axis_index("tp")
@@ -237,18 +237,19 @@
 
     kinds = {"A": (1 - p, n1), "B": (p, fr), "C": (1 - p, ot), "D": (p, fr), "X": (p, xp)}
 
-    def weight(kind, m, h, src=None, cond=None):
+    def weight(kind, m, h, src=None, cond=None, part=None):
         q, to = kinds[kind]
-        rows = pl.ds(h * HK, HK)
+        rows = pl.ds(h * HK, HK) if part is None else pl.ds(h * HK + part * HK // 2, HK // 2)
         sem = w_send.at["ABCDX".index(kind)]
+        arrived = last_recv.at[int(kind == "X")] if part == 1 else w_recv.at[m, s if src is None else src, h]
 
         def copy(width):
-            part = pl.ds(0, width)
+            cols = pl.ds(0, width)
             if src is None:
-                return remote(weights[m].at[rows, columns(q, width)], G.at[m, s, rows, part],
-                              sem, w_recv.at[m, s, h], (to, t))
-            place = G.at[m, src, rows, part]
-            return remote(place, place, sem, w_recv.at[m, src, h], (to, t))
+                return remote(weights[m].at[rows, columns(q, width)], G.at[m, s, rows, cols],
+                              sem, arrived, (to, t))
+            place = G.at[m, src, rows, cols]
+            return remote(place, place, sem, arrived, (to, t))
 
         split(q == c, cond, lambda width: copy(width).start())
 
@@ -266,6 +267,14 @@
             place = G.at[m, src, pl.ds(h * HK, HK), pl.ds(0, width)]
             remote(place, place, w_send.at[0], w_recv.at[m, src, h], (xp, t)).wait_recv()
         split(wide, cond, wait)
+
+    def recv_last(src, x_link, part):
+        sem = last_recv.at[x_link] if part == 1 else w_recv.at[2, src, 1]
+
+        def wait(width):
+            place = G.at[2, src, pl.ds(HK + part * HK // 2, HK // 2), pl.ds(0, width)]
+            remote(place, place, w_send.at[0], sem, (xp, t)).wait_recv()
+        split(wide, None, wait)
 
     def landed(ref, sem):
         remote(ref, ref, w_send.at[0], sem, (s, tc)).wait_recv()
@@ -459,9 +468,11 @@
         recv(m, n1, h, mid)
         weight("X", m, h, src=n1, cond=mid)
         weight("D", m, h, src=n1, cond=mid)
-        if h == 1:
-            weight("C", m, h, cond=mid)
-        weight("B", m, h, cond=mid)
+        if h == 0:
+            weight("B", m, h, cond=mid)
+    for part in (0, 1):
+        weight("B", 2, 1, cond=mid, part=part)
+        weight("C", 2, 1, cond=mid, part=part)
     pass_on(0, 1, ot, outer)
     for g in (tc, td):
         for r in range(2):
@@ -601,14 +612,14 @@
     down(s, 0, 1)
     down(n1, 0, 1)
     cross(s, 0, 1)
-    pass_on(2, 0, ot)
     halves(xp, 0, 1)
     down(xp, 0, 1)
     cross(n1, 0, 1)
-    pass_on(2, 0, fr)
+    pass_on(2, 0, ot)
     halves(n1_x, 0, 1)
     down(n1_x, 0, 1)
     cross(xp, 0, 1)
+    pass_on(2, 0, fr)
     down(ot, 0)
     cross(n1_x, 0, 1)
     down(fr, 0)
@@ -622,7 +633,9 @@
     down(one, 1)
     cross(ot_x, 0)
     lift(xp)
-    pass_on(2, 1, two)
+    for part in (0, 1):
+        recv_last(two, 0, part)
+        weight("X", 2, 1, src=two, part=part)
     halves(fr_x, 0)
     down(fr_x, 0)
     cross(one, 1)
@@ -639,7 +652,8 @@
     lift(fr)
     passing(xp)
     passing(n1_x)
-    halves(two_x, 1)
+    for part in (0, 1):
+        recv_last(two_x, 1, part)
     down(two_x, 1)
     cross(two_x, 1)
     lift(ot_x)
@@ -657,11 +671,9 @@
         for j in range(PER):
             landed(yrecv.at[j, h], y_recv.at[j, h])
             cols = slice((j * 2 + h) * HK, (j * 2 + h + 1) * HK)
-            out_v[:, cols] = (
+            out_ref[:, cols] = (
                 after[t, :, cols].astype(jnp.float32) + (own_sum[j, h] + yrecv[j, h].astype(jnp.float32))
             ).astype(jnp.bfloat16)
-            cp = pltpu.make_async_copy(out_v.at[:, cols], out_hbm.at[:, cols], o_sem.at[0])
-            cp.start()
 
     weights_sent("A", 1)
     weights_sent("B", 1)
@@ -675,7 +687,6 @@
     for j in range(PER):
         for h in (0, 1):
             across(j, h).wait_send()
-    pltpu.make_async_copy(out_v, out_hbm, o_sem.at[0]).wait()
 
 
 def fused(residual, queries, keys, values, documents, sinks, out_weight, norm_gain, gate_weight, up_weight, down_weight):
@@ -695,7 +706,6 @@
         pltpu.VMEM((R, queries.shape[1]), bf),
         pltpu.VMEM((blocks, WINDOW), jnp.int32),
         pltpu.VMEM((T, 1, C), f32),
-        pltpu.VMEM((R, C), bf),
         pltpu.VMEM((3, S, K, W), bf),
         pltpu.VMEM((R + WINDOW, keys.shape[1]), bf),
         pltpu.VMEM((R + WINDOW, keys.shape[1]), bf),
@@ -717,16 +727,16 @@
         pltpu.VMEM((PER, 2, R, HK), f32),
         pltpu.VMEM((PER, 2, R, HK), bf),
         pltpu.VMEM((PER, 2, R, HK), bf),
-        dma((5,)), dma((3, S, 2)), dma((3,)), dma((3,)), dma((8,)),
+        dma((5,)), dma((3, S, 2)), dma((2,)), dma((3,)), dma((3,)), dma((8,)),
         dma((3,)), dma((T + 2,)), dma((3,)), dma((T,)), dma((4, 2)), dma((T, 2)),
         dma((S // 2, 2)), dma((S // 2, 2)), dma((PER, 2)), dma((PER, 2)), dma((S // 2, 2)), dma((S // 2, 2)),
-        dma((1,)), dma((PER, 2)), dma((PER, 2)),
+        dma((PER, 2)), dma((PER, 2)),
     ]
     return pl.pallas_call(
         functools.partial(kernel, S, T, W, N),
-        out_shape=jax.ShapeDtypeStruct((R, C), bf),
+        out_shape=pltpu.VMEM((R, C), bf),
         in_specs=[hbm] * 5 + [pl.BlockSpec(memory_space=pltpu.SMEM)] + [hbm] * 5,
-        out_specs=hbm,
+        out_specs=pl.BlockSpec(memory_space=pltpu.VMEM),
         scratch_shapes=scratch,
         compiler_params=pltpu.CompilerParams(
             collective_id=0, has_side_effects=True, vmem_limit_bytes=60 * 2**20),

time: 120 us -> 118 us (0.983)
  no operation moved by 1% of the time
where the time goes in v5:
time: 118 us
  Pallas kernels  117 us (99%)
    pallas_call x1, Pallas kernels, fused(): pl.pallas_call(functools.partial(kernel, S, T, W, N), out_shape=pltpu.VME...  117 us

profile of v5, /device:TPU:0, one launch (start us, length us, event | category | flops | bytes accessed | tf_op | source)
XLA Modules:
  0.0 118.2 jit_solution(15770405123658135200)
XLA Ops:
  0.0 117.4 %shard_map.109 = bf16[512,512]{1,0:T(8,128)(2,1)S(1)} custom-call(bf16[512,2048]{1,0:T(8,128)(2,1)} %res_hbm.1, bf16[512,256]{1,0:T(8,128)(2,1)} %q_hbm.1, bf16[512,128]{1,0:T(8,128)(2,1)} %k_hbm.1, bf16[512,128]{1,0:T(8,128)(2,1)} %v_hbm.1, s32[4,128]{1,0:T(4,128)} %bitcast.3, f32[4]{0:T(128)} %sink_ref.1, bf16[256,2048]{1,0:T(8,128)(2,1)} %ow_hbm.1, ...), custom_call_target="tpu_custom_call" | custom-call | tf_op jit(solution)/shard_map/pallas_call | solution.py:735
  117.4 0.8 copy.13

commit v6 on v5

--- a/solution.py
+++ b/solution.py
@@ -472,6 +472,7 @@
             weight("B", m, h, cond=mid)
     for part in (0, 1):
         weight("B", 2, 1, cond=mid, part=part)
+    for part in (0, 1):
         weight("C", 2, 1, cond=mid, part=part)
     pass_on(0, 1, ot, outer)
     for g in (tc, td):
@@ -577,6 +578,41 @@
                     back(k, h).start()
                 finish.append(functools.partial(when, kept(k), back(k, h).wait_send))
 
+    def cross_split(k):
+        owned, passed_to = k // PER == t, k // PER == ty
+        j = k % PER
+
+        @pl.when(kept(k))
+        def _():
+            landed(drecv.at[k, 1], d_recv.at[slot(k), 1])
+
+        @pl.when(mid & passed_to)
+        def _():
+            add(nsend, (j, 1), *pair(k, 1, 1))
+            over(j, 1).start()
+
+        @pl.when(outer & kept(k))
+        def _():
+            add(zsend, (k, 1), *pair(k, 1, 1))
+            back(k, 1).start()
+
+        @pl.when(outer & passed_to)
+        def _():
+            add(ysend, (j, 1), *pair(k, 1, 0))
+            across(j, 1).start()
+
+        finish.append(functools.partial(when, mid & passed_to, over(j, 1).wait_send))
+        finish.append(functools.partial(when, (mid & owned) | (outer & kept(k)), back(k, 1).wait_send))
+
+    def lift_split(k):
+        j = k % PER
+
+        @pl.when(mid & (k // PER == t))
+        def _():
+            landed(nrecv.at[j, 1], o_recv.at[j, 1])
+            add(zsend, (k, 1), *pair(k, 1, 1), (nrecv, (j, 1)))
+            back(k, 1).start()
+
     def lift(k):
         j = k % PER
 
@@ -595,10 +631,10 @@
                 landed(zrecv.at[k, h], z_recv.at[slot(k), h])
                 add(own_sum, (k % PER, h), *terms, (zrecv, (k, h)))
 
-    def passing(k):
+    def passing(k, role=True):
         j = k % PER
 
-        @pl.when(k // PER == ty)
+        @pl.when(role & (k // PER == ty))
         def _():
             terms = pair(k, 1, 0)
             landed(zrecv.at[k, 1], z_recv.at[slot(k), 1])
@@ -621,45 +657,47 @@
     cross(xp, 0, 1)
     pass_on(2, 0, fr)
     down(ot, 0)
+    lift(s)
+    lift(n1)
     cross(n1_x, 0, 1)
     down(fr, 0)
     cross(ot, 0)
     halves(ot_x, 0)
     down(ot_x, 0)
+    lift(xp)
     cross(fr, 0)
-    lift(s)
-    lift(n1)
     pass_on(2, 1, one)
     down(one, 1)
     cross(ot_x, 0)
-    lift(xp)
     for part in (0, 1):
         recv_last(two, 0, part)
         weight("X", 2, 1, src=two, part=part)
+    lift(ot)
     halves(fr_x, 0)
     down(fr_x, 0)
-    cross(one, 1)
+    cross_split(one)
+    lift(fr)
     lift(n1_x)
     passing(s)
     passing(n1)
     down(two, 1)
     cross(fr_x, 0)
-    cross(two, 1)
-    lift(ot)
+    cross_split(two)
+    lift(ot_x)
     halves(one_x, 1)
     down(one_x, 1)
     cross(one_x, 1)
-    lift(fr)
+    lift_split(one)
+    lift(fr_x)
     passing(xp)
     passing(n1_x)
     for part in (0, 1):
         recv_last(two_x, 1, part)
     down(two_x, 1)
     cross(two_x, 1)
-    lift(ot_x)
-    lift(fr_x)
-    passing(one)
-    passing(two)
+    lift_split(two)
+    passing(one, mid)
+    passing(two, mid)
     passing(one_x)
     passing(two_x)
     for k in (s, n1, xp, n1_x):

time: 118 us -> 118 us (level); the launches traced: 118 us -> 116 us
  Pallas kernels: 117 us -> 115 us
    pallas_call x1, Pallas kernels: 117 us -> 115 us  [fused(): pl.pallas_call(functools.partial(kernel, S, T, W, N), out_shape=pltpu.VME...]
where the time goes in v6:
time: 118 us; the launch traced here: 116 us
  Pallas kernels  115 us (97%)
    pallas_call x1, Pallas kernels, fused(): pl.pallas_call(functools.partial(kernel, S, T, W, N), out_shape=pltpu.VME...  115 us

profile of v6, /device:TPU:0, one launch (start us, length us, event | category | flops | bytes accessed | tf_op | source)
XLA Modules:
  0.0 115.7 jit_solution(17642597191044461378)
XLA Ops:
  0.0 114.9 %shard_map.109 = bf16[512,512]{1,0:T(8,128)(2,1)S(1)} custom-call(bf16[512,2048]{1,0:T(8,128)(2,1)} %res_hbm.1, bf16[512,256]{1,0:T(8,128)(2,1)} %q_hbm.1, bf16[512,128]{1,0:T(8,128)(2,1)} %k_hbm.1, bf16[512,128]{1,0:T(8,128)(2,1)} %v_hbm.1, s32[4,128]{1,0:T(4,128)} %bitcast.3, f32[4]{0:T(128)} %sink_ref.1, bf16[256,2048]{1,0:T(8,128)(2,1)} %ow_hbm.1, ...), custom_call_target="tpu_custom_call" | custom-call | tf_op jit(solution)/shard_map/pallas_call | solution.py:773
  114.9 0.8 copy.13

commit v7 on v6

--- a/solution.py
+++ b/solution.py
@@ -495,7 +495,6 @@
     gate_up(fr_x, 0, 2 * R)
     for m, h in GU:
         recv(m, ot_x, h)
-    pass_on(2, 1, n1, outer)
     gate_up(ot_x, 0, 2 * R)
 
     def act(r, carry):
@@ -613,10 +612,10 @@
             add(zsend, (k, 1), *pair(k, 1, 1), (nrecv, (j, 1)))
             back(k, 1).start()
 
-    def lift(k):
+    def lift(k, role=True):
         j = k % PER
 
-        @pl.when(k // PER == t)
+        @pl.when(role & (k // PER == t))
         def _():
             terms = pair(k, 0, 1)
             landed(nrecv.at[j, 0], o_recv.at[j, 0])
@@ -646,6 +645,7 @@
             recv(2, src, h)
 
     down(s, 0, 1)
+    pass_on(2, 1, n1, outer)
     down(n1, 0, 1)
     cross(s, 0, 1)
     halves(xp, 0, 1)
@@ -672,23 +672,25 @@
     for part in (0, 1):
         recv_last(two, 0, part)
         weight("X", 2, 1, src=two, part=part)
-    lift(ot)
+    lift(ot, mid)
     halves(fr_x, 0)
     down(fr_x, 0)
     cross_split(one)
-    lift(fr)
+    lift(fr, mid)
+    lift(ot, outer)
     lift(n1_x)
     passing(s)
     passing(n1)
     down(two, 1)
     cross(fr_x, 0)
     cross_split(two)
-    lift(ot_x)
+    lift(ot_x, mid)
     halves(one_x, 1)
     down(one_x, 1)
     cross(one_x, 1)
     lift_split(one)
-    lift(fr_x)
+    lift(fr_x, mid)
+    lift(fr, outer)
     passing(xp)
     passing(n1_x)
     for part in (0, 1):
@@ -696,6 +698,8 @@
     down(two_x, 1)
     cross(two_x, 1)
     lift_split(two)
+    lift(ot_x, outer)
+    lift(fr_x, outer)
     passing(one, mid)
     passing(two, mid)
     passing(one_x)

time: 118 us -> 118 us (level)
  no operation moved by 1% of the time
where the time goes in v7:
time: 118 us; the launch traced here: 116 us
  Pallas kernels  115 us (97%)
    pallas_call x1, Pallas kernels, fused(): pl.pallas_call(functools.partial(kernel, S, T, W, N), out_shape=pltpu.VME...  115 us

profile of v7, /device:TPU:0, one launch (start us, length us, event | category | flops | bytes accessed | tf_op | source)
XLA Modules:
  0.0 115.7 jit_solution(9362421880399532844)
XLA Ops:
  0.0 114.9 %shard_map.109 = bf16[512,512]{1,0:T(8,128)(2,1)S(1)} custom-call(bf16[512,2048]{1,0:T(8,128)(2,1)} %res_hbm.1, bf16[512,256]{1,0:T(8,128)(2,1)} %q_hbm.1, bf16[512,128]{1,0:T(8,128)(2,1)} %k_hbm.1, bf16[512,128]{1,0:T(8,128)(2,1)} %v_hbm.1, s32[4,128]{1,0:T(4,128)} %bitcast.3, f32[4]{0:T(128)} %sink_ref.1, bf16[256,2048]{1,0:T(8,128)(2,1)} %ow_hbm.1, ...), custom_call_target="tpu_custom_call" | custom-call | tf_op jit(solution)/shard_map/pallas_call | solution.py:777
  114.9 0.8 copy.13
